TPU v7x, 256 devices: a 4x2x16 block of a 4x16x16 slice. The times are simulated.
256 devices in a mesh: grp: 2 (over y), ep: 32 (over z, core), tp: 4 (over x).
Axes of the slice: x: 4, y: 2, z: 16, core: 2. Of those that a mesh axis runs over, the one named last changes fastest.
The devices are a block of a 4x16x16 slice.
Arguments:
- mixer_tokens: bfloat16 [32768, 2048], P(('grp', 'ep', 'tp')), parts along dimension 0, may hold values from -6 to 6
- mixer_gain: bfloat16 [2048], replicated, may hold values from 0.099609375 to 1.8984375
- in_weight: bfloat16 [2048, 2048], P(None, 'tp'), may hold values from -0.125 to 0.125
- group_weight: bfloat16 [4, 512, 512], P('tp'), may hold values from -0.25 to 0.25
- channel_scale: bfloat16 [2048], P('tp'), may hold values from 0.099609375 to 1.8984375
- out_weight: bfloat16 [2048, 2048], P('tp'), may hold values from -0.125 to 0.125
- expert_tokens: bfloat16 [32768, 2048], P(('grp', 'ep', 'tp')), parts along dimension 0, may hold values from -6 to 6
- expert_gain: bfloat16 [2048], replicated, may hold values from 0.099609375 to 1.8984375
- route_ids: int32 [32768, 2], P(('grp', 'ep', 'tp')), parts along dimension 0, may hold values from 0 to 31, all different within a row; in each aligned block of 128 rows (0 to 127, 128 to 255, ...) at most 16 rows name the same one
- route_weights: float32 [32768, 2], P(('grp', 'ep', 'tp')), parts along dimension 0, may hold values from 0.1 to 1
- gate_weight: bfloat16 [32, 2048, 1024], P('ep', None, 'tp'), may hold values from -0.125 to 0.125
- up_weight: bfloat16 [32, 2048, 1024], P('ep', None, 'tp'), may hold values from -0.125 to 0.125
- down_weight: bfloat16 [32, 1024, 2048], P('ep', 'tp'), may hold values from -0.1875 to 0.1875
Outputs:
- mixed_tokens: bfloat16 [32768, 2048], P(('grp', 'ep', 'tp')), parts along dimension 0
- expert_mix: bfloat16 [32768, 2048], P(('grp', 'ep', 'tp')), parts along dimension 0
There are 2 independent parts, one for each index of `grp`. A program takes and returns all parts, laid end to end along the dimension named above; an argument that names none is the same for every part. Nothing has to cross between parts.
Inputs may be any that keep to these rules, and one draw needn't show every extreme that they name: `route_ids`: each row names 2 different experts; in the rows of one device no expert is named more than 16 times, and one expert exactly 16 times in the rows of some device.
All inputs are finite; a program needn't handle non-finite values.
Results may differ from a plain program's by a relative error of at most 0.015.
Values may be sent and summed in bfloat16 or wider, within the bound.
A program may use at most 128 MiB of HBM per device.

v0:
```python
import jax
import jax.numpy as jnp
from jax import lax
from jax.sharding import PartitionSpec as P

WINDOW_MAX = 16


def from_everyone(value, axis):
    devices = lax.axis_size(axis)
    return lax.all_to_all(
        jnp.broadcast_to(value[None], (devices, *value.shape)), axis, 0, 0, tiled=True
    )


def joined_along(tiles, dim):
    tiles = jnp.moveaxis(tiles, 0, dim)
    shape = tiles.shape
    return tiles.reshape(*shape[:dim], shape[dim] * shape[dim + 1], *shape[dim + 2 :])


def collect(value, axis, dim):
    tiles = from_everyone(value, axis)
    return joined_along(tiles, dim)


def shifted(value, axis, by):
    devices = lax.axis_size(axis)
    pairs = [(i, i + by) for i in range(devices) if 0 <= i + by < devices]
    return lax.ppermute(value, axis, pairs)


def cut_along(value, dim, devices):
    shape = value.shape
    tiles = value.reshape(*shape[:dim], devices, shape[dim] // devices, *shape[dim + 1 :])
    return jnp.moveaxis(tiles, dim, 0)


def sent_and_summed(value, axis, dim):
    tiles = cut_along(value, dim, lax.axis_size(axis))
    arrived = lax.all_to_all(tiles, axis, split_axis=0, concat_axis=0, tiled=True)
    return arrived.astype(jnp.float32).sum(axis=0)


def exchange_in_groups(value, axis, split_dim, concat_dim, work, item_dim, out_dim):

    def moved(group):
        return lax.all_to_all(group, axis, split_axis=split_dim, concat_axis=concat_dim, tiled=True)

    items = jax.tree.leaves(value)[0].shape[item_dim]
    ends = [items * k // 2 for k in range(2 + 1)] if items % 2 == 0 else [0, items]
    groups = [
        jax.tree.map(lambda a: lax.slice_in_dim(a, low, high, axis=item_dim), value)
        for low, high in zip(ends, ends[1:])
    ]
    arrived = [moved(group) for group in groups]
    made = [work(group) for group in arrived]
    return jax.tree.map(lambda *parts: jnp.concatenate(parts, axis=out_dim), *made)


def rms_rows(rows, gain):
    values = rows.astype(jnp.float32)
    scaled = values * lax.rsqrt(jnp.mean(values * values, axis=-1, keepdims=True) + 1e-06)
    return (scaled * gain.astype(jnp.float32)).astype(jnp.bfloat16)


def expert_hidden(rows, w_gate, w_up):
    gate = jnp.dot(rows, w_gate, preferred_element_type=jnp.float32)
    upper = jnp.dot(rows, w_up, preferred_element_type=jnp.float32)
    return (jax.nn.silu(gate) * upper).astype(jnp.bfloat16)


def local(
    mixer_tokens,
    mixer_gain,
    in_weight,
    group_weight,
    channel_scale,
    out_weight,
    expert_tokens,
    expert_gain,
    route_ids,
    route_weights,
    gate_weight,
    up_weight,
    down_weight,
):
    normed = rms_rows(mixer_tokens, mixer_gain)
    pooled_in = jnp.dot(
        collect(normed, "tp", 0), in_weight, preferred_element_type=jnp.float32
    ).astype(jnp.bfloat16)
    block_rows = pooled_in.shape[0]
    rim_rows = shifted(pooled_in[block_rows - WINDOW_MAX :], "ep", 1)
    values = pooled_in.astype(jnp.float32)
    extended = jnp.concatenate([rim_rows.astype(jnp.float32), values], axis=0)
    window = jnp.left_shift(jnp.int32(2), lax.axis_index("tp"))
    sums = extended
    span = 1
    total = jnp.zeros_like(values)
    for level in range(WINDOW_MAX.bit_length() - 1):
        sums = sums[span:] + sums[:-span]
        span = span * 2
        total = total + jnp.where(window == span, sums[sums.shape[0] - block_rows :], 0.0)
    positions = lax.axis_index("ep") * block_rows + lax.iota(jnp.int32, block_rows) + 1
    counts = jnp.minimum(positions, window).astype(jnp.float32)
    pooled = (total / counts[:, None] - values).astype(jnp.bfloat16)
    grouped = (
        jnp.dot(pooled, group_weight[0], preferred_element_type=jnp.float32)
        * channel_scale.astype(jnp.float32)
    ).astype(jnp.bfloat16)
    rows = grouped
    mixed_tokens = sent_and_summed(
        jnp.dot(rows, out_weight, preferred_element_type=jnp.float32).astype(jnp.bfloat16), "tp", 0
    ).astype(jnp.bfloat16)
    expert_in = rms_rows(expert_tokens, expert_gain)
    shares = route_weights / jnp.sum(route_weights, axis=1, keepdims=True)
    rows_here, top_k = route_ids.shape
    width = expert_in.shape[1]
    n_experts = lax.axis_size("ep") * gate_weight.shape[0]
    capacity = 4 * rows_here // n_experts
    flat_ids = route_ids.reshape(rows_here * top_k)
    one_hot = (flat_ids[:, None] == jnp.arange(n_experts, dtype=jnp.int32)[None, :]).astype(
        jnp.int32
    )
    before = jnp.cumsum(one_hot, axis=0) - one_hot
    slots = jnp.sum(before * one_hot, axis=1)
    targets = flat_ids * capacity + slots
    placement = (
        targets.reshape(rows_here, top_k)[None, :, :]
        == jnp.arange(n_experts * capacity, dtype=jnp.int32)[:, None, None]
    )
    dispatch = jnp.any(placement, axis=2).astype(jnp.bfloat16)
    outgoing = jnp.dot(dispatch, expert_in, preferred_element_type=jnp.float32).astype(jnp.bfloat16)
    outgoing = outgoing.reshape(n_experts, capacity, width)

    def serve_sectioned(arrived):
        sources, held, _ = arrived.shape
        flat = arrived.reshape(sources * held, width)
        hidden = expert_hidden(
            lax.all_gather(flat, "tp", axis=0, tiled=True), gate_weight[0], up_weight[0]
        )
        rows = lax.slice_in_dim(hidden, 0, sources * held * lax.axis_size("tp"), axis=0)
        summed = lax.psum_scatter(
            jnp.dot(rows, down_weight[0], preferred_element_type=jnp.float32).astype(jnp.bfloat16),
            "tp",
            scatter_dimension=0,
            tiled=True,
        ).astype(jnp.float32)
        return lax.all_to_all(
            summed.reshape(sources, held, width).astype(jnp.bfloat16),
            "ep",
            split_axis=0,
            concat_axis=0,
            tiled=True,
        ).astype(jnp.float32)

    expert_out = exchange_in_groups(outgoing, "ep", 0, 0, serve_sectioned, 1, 1)
    flat_out = expert_out.reshape(n_experts * capacity, width)
    picked = jnp.take(flat_out, targets, axis=0).reshape(rows_here, top_k, width)
    expert_mix = jnp.sum(picked * shares[:, :, None], axis=1).astype(jnp.bfloat16)
    return (mixed_tokens, expert_mix)


def solution(mesh):
    placed = (
        P(("grp", "ep", "tp"), None),
        P(),
        P(None, "tp"),
        P("tp", None, None),
        P("tp"),
        P("tp", None),
        P(("grp", "ep", "tp"), None),
        P(),
        P(("grp", "ep", "tp"), None),
        P(("grp", "ep", "tp"), None),
        P("ep", None, "tp"),
        P("ep", None, "tp"),
        P("ep", "tp", None),
    )
    return jax.shard_map(
        local,
        mesh=mesh,
        in_specs=placed,
        out_specs=(P(("grp", "ep", "tp"), None), P(("grp", "ep", "tp"), None)),
        check_vma=False,
    )
```

profile of v0, /device:TPU:45, one launch (start us, length us, event | category | flops | bytes accessed | tf_op | source)
XLA Modules:
  0.0 454.4 jit_solution(7608851029754211037)
XLA Ops:
  7.3 0.9 copy.29
  8.3 0.1 reshape.128
  8.5 0.6 reduce-window.6
  9.1 0.2 slice_reduce_fusion
  9.4 0.1 reduce_sum.64
  9.6 0.7 compare_and_fusion
  10.4 0.7 convert_element_type.100
  11.1 1.2 fusion.7
  12.3 1.8 convolution_convert_fusion.2
  14.1 0.2 fusion.72
  14.3 80.0 %all_to_all.30 = bf16[32,8,2048]{2,1,0:T(8,128)(2,1)} all-to-all(bf16[32,8,2048]{2,1,0:T(8,128)(2,1)S(1)} %get-tuple-element.4), channel_id=1, replica_groups=mesh['grp'=2,'ep'=32,'tp'=4] {'ep'}, dimensions={0} | all-to-all | bytes 2097152 | tf_op jit(solution)/shard_map/all_to_all | solution.py:48
  94.5 59.7 %all_to_all.31 = bf16[32,8,2048]{2,1,0:T(8,128)(2,1)} all-to-all(bf16[32,8,2048]{2,1,0:T(8,128)(2,1)S(1)} %get-tuple-element.5), channel_id=1, replica_groups=mesh['grp'=2,'ep'=32,'tp'=4] {'ep'}, dimensions={0} | all-to-all | bytes 2097152 | tf_op jit(solution)/shard_map/all_to_all | solution.py:48
  154.4 4.9 %fusion.24 = f32[1024,256]{1,0:T(8,128)} fusion(bf16[1024,2048]{1,0:T(8,128)(2,1)} %all-gather.3.cloned.1.call-done, bf16[1,2048,256]{2,1,0:T(8,128)(2,1)} %param.23), kind=kOutput, calls=%fused_computation.45 | convolution fusion | flops 1073741824 | bytes 6291456 | tf_op jit(solution)/shard_map/dot_general | solution.py:68
  159.2 9.4 %convolution_convert_fusion.1 = bf16[1024,2048]{1,0:T(8,128)(2,1)} fusion(bf16[1024,2048]{1,0:T(8,128)(2,1)} %all-gather.3.cloned.1.call-done, bf16[1,256,2048]{2,1,0:T(8,128)(2,1)S(1)} %copy-done.10, bf16[1,2048,256]{2,1,0:T(8,128)(2,1)} %param.24, f32[1024,256]{1,0:T(8,128)} %fusion.24), kind=kOutput, calls=%fused_computation.2 | convolution fusion | flops 2151153664 | bytes 11534336 | tf_op jit(solution)/shard_map/dot_general | solution.py:144
  168.7 0.6 copy-done.5
  169.3 0.4 copy-done.3
  169.7 0.2 fusion.4
  169.9 0.2 fusion.6
  170.1 1.6 broadcast_in_dim.16
  171.7 4.6 %all-to-all-start = ((bf16[4,128,2048]{2,1,0:T(8,128)(2,1)}), bf16[4,128,2048]{2,1,0:T(8,128)(2,1)}, u32[]{:S(2)}, u32[]{:S(2)}) async-start(bf16[4,128,2048]{2,1,0:T(8,128)(2,1)} %broadcast_in_dim.16), calls=%async_computation | async-start | bytes 4194304 | tf_op jit(solution)/shard_map/all_to_all | solution.py:11
  176.3 0.2 reduce-scatter.5.cloned.1.call-start
  176.5 42.0 %all-gather.5.cloned.1.call-done = bf16[1024,2048]{1,0:T(8,128)(2,1)} async-done(((bf16[256,2048]{1,0:T(8,128)(2,1)}), bf16[1024,2048]{1,0:T(8,128)(2,1)}) %all-gather.5.cloned.1.call-update) | async-done | bytes 4194320 | tf_op jit(solution)/shard_map/all_gather | solution.py:140
  218.5 4.5 fusion.22
  223.0 9.4 %convolution_convert_fusion = bf16[1024,2048]{1,0:T(8,128)(2,1)} fusion(bf16[1024,2048]{1,0:T(8,128)(2,1)} %all-gather.5.cloned.1.call-done, bf16[1,256,2048]{2,1,0:T(8,128)(2,1)} %param.25, bf16[1,2048,256]{2,1,0:T(8,128)(2,1)} %param.24, f32[1024,256]{1,0:T(8,128)} %fusion.22), kind=kOutput, calls=%fused_computation.1 | convolution fusion | flops 2151153664 | bytes 11534336 | tf_op jit(solution)/shard_map/dot_general | solution.py:144
  232.5 4.5 fusion.74
  237.0 7.0 %collective-permute-start = (bf16[16,512]{1,0:T(8,128)(2,1)S(1)}, bf16[16,512]{1,0:T(8,128)(2,1)S(1)}, u32[]{:S(2)}, u32[]{:S(2)}) collective-permute-start(bf16[16,512]{1,0:T(8,128)(2,1)S(1)} %slice.70), channel_id=1, source_target_pairs={{0,4},{4,8},{8,12},{12,16},{16,20},{20,24},{24,28},{28,32},{32,36}... | collective-permute-start | bytes 49160 | tf_op jit(solution)/shard_map/ppermute | solution.py:30
  244.0 0.8 collective-permute-done
  244.8 1.8 fusion.3
  246.6 0.1 slice_add_fusion.1
  246.8 1.0 copy-done.1
  247.8 0.1 slice_add_fusion
  247.9 1.7 fusion.73
  249.7 6.0 %convolution_convert_fusion.3 = bf16[512,2048]{1,0:T(8,128)(2,1)} fusion(bf16[512,2048]{1,0:T(8,128)(2,1)S(1)} %copy-done, f32[513,512]{1,0:T(8,128)} %get-tuple-element.7, f32[513,512]{1,0:T(8,128)} %get-tuple-element.6, f32[521,512]{1,0:T(8,128)} %copy-done.2, f32[525,512]{1,0:T(8,128)} %copy-done.1, f32[527,512]{1,0:T(8,128)S(1)} %fusion.3, ...), kind=kOutput, calls=%fused_computation.4 | convolution fusion | flops 1346895872 | bytes 10489860 | tf_op jit(solution)/shard_map/dot_general | solution.py:113
  255.6 42.2 %all_to_all.32 = bf16[4,128,2048]{2,1,0:T(8,128)(2,1)} all-to-all(bf16[4,128,2048]{2,1,0:T(8,128)(2,1)} %bitcast.63), channel_id=1, replica_groups=mesh['grp'=2,'ep'=32,'tp'=4] {'tp'}, dimensions={0} | all-to-all | bytes 4194304 | tf_op jit(solution)/shard_map/all_to_all | solution.py:41
  297.8 0.6 reduce-scatter.3.cloned.1.call-done
  298.5 13.6 %all-to-all-start.3 = ((bf16[32,8,2048]{2,1,0:T(8,128)(2,1)}), bf16[32,8,2048]{2,1,0:T(8,128)(2,1)S(1)}, u32[]{:S(2)}, u32[]{:S(2)}) async-start(bf16[32,8,2048]{2,1,0:T(8,128)(2,1)} %bitcast.64), calls=%async_computation.4 | async-start | bytes 2097152 | tf_op jit(solution)/shard_map/all_to_all | solution.py:149
  312.1 41.8 %reduce-scatter.5.cloned.1.call-done = bf16[256,2048]{1,0:T(8,128)(2,1)} async-done(((bf16[1024,2048]{1,0:T(8,128)(2,1)}), bf16[256,2048]{1,0:T(8,128)(2,1)}) %reduce-scatter.5.cloned.1.call-update) | async-done | bytes 1048592 | tf_op jit(solution)/shard_map/reduce_scatter | solution.py:143
  353.9 13.7 %all-to-all-done.3 = bf16[32,8,2048]{2,1,0:T(8,128)(2,1)S(1)} async-done(((bf16[32,8,2048]{2,1,0:T(8,128)(2,1)}), bf16[32,8,2048]{2,1,0:T(8,128)(2,1)S(1)}, u32[]{:S(2)}, u32[]{:S(2)}) %all-to-all-start.3) | async-done | bytes 1048608 | tf_op jit(solution)/shard_map/all_to_all | solution.py:149
  367.6 5.1 %all-to-all-start.5 = ((bf16[32,8,2048]{2,1,0:T(8,128)(2,1)}), bf16[32,8,2048]{2,1,0:T(8,128)(2,1)}, u32[]{:S(2)}, u32[]{:S(2)}) async-start(bf16[32,8,2048]{2,1,0:T(8,128)(2,1)} %bitcast.65), calls=%async_computation.7 | async-start | bytes 2097152 | tf_op jit(solution)/shard_map/all_to_all | solution.py:149
  372.8 0.1 mul.114
  373.0 0.1 copy.33
  373.3 2.9 reduce_sum.62
  376.2 52.0 %all-to-all-done.5 = bf16[32,8,2048]{2,1,0:T(8,128)(2,1)} async-done(((bf16[32,8,2048]{2,1,0:T(8,128)(2,1)}), bf16[32,8,2048]{2,1,0:T(8,128)(2,1)}, u32[]{:S(2)}, u32[]{:S(2)}) %all-to-all-start.5) | async-done | bytes 1048608 | tf_op jit(solution)/shard_map/all_to_all | solution.py:149
  428.3 1.4 pad_maximum_fusion
  429.6 2.6 bitcast_convert_fusion
  432.2 5.8 %gather_fusion = f32[256,2048]{1,0:T(8,128)} fusion(f32[512,2048]{1,0:T(8,128)} %bitcast_convert_fusion, s32[1024]{0:T(1024)S(1)} %pad_clamp_fusion), kind=kCustom, calls=%fused_computation | custom fusion | bytes 4195328 | tf_op jit(solution)/shard_map/jit(_take)/gather | solution.py:159
  438.0 3.5 gather.7
  441.5 6.4 %multiply_reduce_fusion = bf16[128,2048]{1,0:T(8,128)(2,1)} fusion(f32[128,2,2048]{2,1,0:T(2,128)} %gather.7, pred[128,2]{1,0:T(8,128)(4,1)S(1)} %copy.33, f32[128,2]{1,0:T(8,128)S(1)} %copy.35), kind=kLoop, calls=%fused_computation.7 | loop fusion | flops 1310720 | bytes 2622720 | tf_op jit(solution)/shard_map/reduce_sum | solution.py:160
  (49 shorter events, 1.2 us)
Async XLA Ops:
  7.2 242.5 %copy-start = (bf16[512,2048]{1,0:T(8,128)(2,1)S(1)}, bf16[512,2048]{1,0:T(8,128)(2,1)}, u32[]{:S(2)}) copy-start(bf16[512,2048]{1,0:T(8,128)(2,1)} %param.18) | copy-start | bytes 6291460
  7.2 147.2 %all-gather.3.cloned.1.call-start = ((), (), s32[]{:S(2)}) async-start(), calls=%async_computation.8 | async-start | bytes 5242880 | tf_op jit(solution)/shard_map/all_gather | solution.py:140
  94.4 124.1 %all-gather.5.cloned.1.call-start = ((), (), s32[]{:S(2)}) async-start(), calls=%async_computation.10 | async-start | bytes 5242880 | tf_op jit(solution)/shard_map/all_gather | solution.py:140
  154.2 5.0 %copy-start.10 = (bf16[1,256,2048]{2,1,0:T(8,128)(2,1)S(1)}, bf16[1,256,2048]{2,1,0:T(8,128)(2,1)}, u32[]{:S(2)}) copy-start(bf16[1,256,2048]{2,1,0:T(8,128)(2,1)} %param.25) | copy-start | bytes 3145732
  154.3 144.2 %reduce-scatter.3.cloned.1.call-start = ((), (), s32[]{:S(2)}) async-start(), calls=%async_computation.9 | async-start | bytes 5242880 | tf_op jit(solution)/shard_map/reduce_scatter | solution.py:143
  168.6 0.7 copy-start.5
  168.6 1.1 copy-start.3
  171.7 46.9 %copy-start.9 = (bf16[1,2048,256]{2,1,0:T(8,128)(2,1)S(1)}, bf16[1,2048,256]{2,1,0:T(8,128)(2,1)}, u32[]{:S(2)}) copy-start(bf16[1,2048,256]{2,1,0:T(8,128)(2,1)} %param.23) | copy-start | bytes 3145732
  171.7 60.8 %all-to-all-start = ((bf16[4,128,2048]{2,1,0:T(8,128)(2,1)}), bf16[4,128,2048]{2,1,0:T(8,128)(2,1)}, u32[]{:S(2)}, u32[]{:S(2)}) async-start(bf16[4,128,2048]{2,1,0:T(8,128)(2,1)} %broadcast_in_dim.16), calls=%async_computation | async-start | bytes 4194304 | tf_op jit(solution)/shard_map/all_to_all | solution.py:11
  176.3 177.7 %reduce-scatter.5.cloned.1.call-start = ((), (), s32[]{:S(2)}) async-start(), calls=%async_computation.11 | async-start | bytes 5242880 | tf_op jit(solution)/shard_map/reduce_scatter | solution.py:143
  232.5 11.5 %copy-start.7 = (bf16[512]{0:T(512)(128)(2,1)S(1)}, bf16[512]{0:T(512)(128)(2,1)}, u32[]{:S(2)}) copy-start(bf16[512]{0:T(512)(128)(2,1)} %param.17) | copy-start | bytes 3076
  237.0 7.8 %copy-start.8 = (bf16[512,512]{1,0:T(8,128)(2,1)}, bf16[512,512]{1,0:T(8,128)(2,1)S(1)}, u32[]{:S(2)}) copy-start(bf16[512,512]{1,0:T(8,128)(2,1)S(1)} %get-tuple-element.9) | copy-start | bytes 1572868
  237.0 7.8 %collective-permute-start = (bf16[16,512]{1,0:T(8,128)(2,1)S(1)}, bf16[16,512]{1,0:T(8,128)(2,1)S(1)}, u32[]{:S(2)}, u32[]{:S(2)}) collective-permute-start(bf16[16,512]{1,0:T(8,128)(2,1)S(1)} %slice.70), channel_id=1, source_target_pairs={{0,4},{4,8},{8,12},{12,16},{16,20},{20,24},{24,28},{28,32},{32,36}... | collective-permute-start | bytes 49160 | tf_op jit(solution)/shard_map/ppermute | solution.py:30
  246.8 1.0 copy-start.1
  247.9 1.7 copy-start.2
  298.5 74.2 %copy-start.4 = (s32[128,2]{0,1:T(2,128)S(1)}, s32[128,2]{0,1:T(2,128)}, u32[]{:S(2)}) copy-start(s32[128,2]{0,1:T(2,128)} %param.21) | copy-start | bytes 3076
  298.5 74.6 %copy-start.6 = (f32[128,2]{0,1:T(2,128)S(1)}, f32[128,2]{0,1:T(2,128)}, u32[]{:S(2)}) copy-start(f32[128,2]{0,1:T(2,128)} %param.22) | copy-start | bytes 3076
  298.5 69.1 %all-to-all-start.3 = ((bf16[32,8,2048]{2,1,0:T(8,128)(2,1)}), bf16[32,8,2048]{2,1,0:T(8,128)(2,1)S(1)}, u32[]{:S(2)}, u32[]{:S(2)}) async-start(bf16[32,8,2048]{2,1,0:T(8,128)(2,1)} %bitcast.64), calls=%async_computation.4 | async-start | bytes 2097152 | tf_op jit(solution)/shard_map/all_to_all | solution.py:149
  367.6 60.7 %all-to-all-start.5 = ((bf16[32,8,2048]{2,1,0:T(8,128)(2,1)}), bf16[32,8,2048]{2,1,0:T(8,128)(2,1)}, u32[]{:S(2)}, u32[]{:S(2)}) async-start(bf16[32,8,2048]{2,1,0:T(8,128)(2,1)} %bitcast.65), calls=%async_computation.7 | async-start | bytes 2097152 | tf_op jit(solution)/shard_map/all_to_all | solution.py:149
Sparse Core Ops, SparseCore 0:
  94.6 44.8 all-gather.2
  154.4 64.1 all-gather.4
  221.1 77.3 reduce-scatter.2
  300.9 52.9 reduce-scatter.4
where the time goes:
time: 459 us; the launch traced here: 454 us
  blocking collectives  182 us (40%)
  waiting for transfers between devices  151 us (33%)
  matrix products  40.4 us (9%)
  starting transfers between devices  30.7 us (7%)
  other arithmetic  19.2 us (4%)
  local copies, waits for them, and re-layouts  16.9 us (4%)
  between operations  14.1 us (3%)
    all_to_all x2, blocking collectives, moved(): lax.all_to_all(group, axis, split_axis=split_dim, concat_axis=concat_dim,...  140 us
    all_to_all x2, waiting for transfers between devices, serve_sectioned(): lax.all_to_all(summed.reshape(sources, held, width).astype(jnp.bfloat16),...  65.7 us
    reduce_scatter x2, waiting for transfers between devices, serve_sectioned(): lax.psum_scatter(jnp.dot(rows, down_weight[0], preferred_element_type=jnp...  42.4 us
    all_to_all x1, blocking collectives, sent_and_summed(): lax.all_to_all(tiles, axis, split_axis=0, concat_axis=0, tiled=True)  42.2 us
    all_gather x2, waiting for transfers between devices, serve_sectioned(): lax.all_gather(flat, 'tp', axis=0, tiled=True)  42 us
    dot_general x2, matrix products, serve_sectioned(): jnp.dot(rows, down_weight[0], preferred_element_type=jnp.float32)  18.8 us
    all_to_all x2, starting transfers between devices, serve_sectioned(): lax.all_to_all(summed.reshape(sources, held, width).astype(jnp.bfloat16),...  18.7 us
    dot_general x2, matrix products, expert_hidden(): gate = jnp.dot(rows, w_gate, preferred_element_type=jnp.float32)  9.34 us
  transfers between devices with their start and end apart: 8, of which 6 were waited for; matrix products, arithmetic and copies ran while one was open for 11% of the time, Pallas kernels for 0%

commit v1 on v0

v1 whole, which is shorter than its diff:
```python
import functools

import jax
import jax.numpy as jnp
from jax import lax
from jax.experimental import pallas as pl
from jax.experimental.pallas import tpu as pltpu
from jax.sharding import PartitionSpec as P

MESH = pl.DeviceIdType.MESH
F32 = jnp.float32
BF16 = jnp.bfloat16
WINDOW_MAX = 16


def dot(a, b):
    return jnp.dot(a, b, preferred_element_type=F32)


def rms_rows(rows, gain):
    values = rows.astype(F32)
    scaled = values * lax.rsqrt(jnp.mean(values * values, axis=-1, keepdims=True) + 1e-06)
    return (scaled * gain.astype(F32)).astype(BF16)


def far_first(j, n):
    return n // 2 + (1 - 2 * (j % 2)) * ((j + 1) // 2)


def kernel(
    n_ep, n_tp, cap,
    mtok, mgain, inw, gw, scale, ow, etok, egain, ids, ids_t, shares, gate, up, down,
    mixed_out, expert_out,
    xin, out_buf, in_buf, res_buf, ret_buf, acc, wg, wu, wd,
    mrows, normed, inw_v, gw_v, ow_v, ext, part_buf, part_in, mixed_v, expert_v,
    load_sem, tok_send, tok_recv, ret_send, ret_recv, w_send, w_recv,
    ag_send, ag_recv, halo_send, halo_recv, rs_send, rs_recv, out_sem,
):
    ep = lax.axis_index("ep")
    tp = lax.axis_index("tp")
    rows, width = etok.shape
    n_slots = n_ep * cap
    half = n_ep // 2
    right, left = (tp + 1) % n_tp, (tp + n_tp - 1) % n_tp
    depth = down.shape[1]

    barrier = pltpu.get_barrier_semaphore()

    @pl.loop(1, n_ep)
    def _(r):
        pl.semaphore_signal(
            barrier, inc=1, device_id={"ep": (ep + r) % n_ep}, device_id_type=MESH
        )

    for r in range(1, n_tp):
        pl.semaphore_signal(
            barrier, inc=1, device_id={"tp": (tp + r) % n_tp}, device_id_type=MESH
        )

    loads = [
        pltpu.make_async_copy(src, dst, load_sem.at[i])
        for i, (src, dst) in enumerate(
            [
                (gate.at[0], wg.at[0]),
                (up.at[0], wu.at[0]),
                (down.at[0], wd.at[0]),
                (mtok, mrows),
                (inw, inw_v),
                (gw.at[0], gw_v),
                (ow, ow_v),
            ]
        )
    ]
    for load in loads:
        load.start()

    def weights(i, src, dst, to):
        return pltpu.make_async_remote_copy(
            src_ref=src,
            dst_ref=dst,
            send_sem=w_send.at[i],
            recv_sem=w_recv.at[i],
            device_id={"tp": to},
            device_id_type=MESH,
        )

    low, high = pl.ds(0, depth // 2), pl.ds(depth // 2, depth // 2)
    to_right = [
        weights(0, gate.at[0], wg.at[1], right),
        weights(1, down.at[0], wd.at[1], right),
        weights(2, up.at[0], wu.at[1], right),
    ]
    to_left = [
        weights(3, up.at[0], wu.at[2], left),
        weights(4, down.at[0], wd.at[2], left),
        weights(5, gate.at[0], wg.at[2], left),
    ]
    on_right = [
        weights(6, wg.at[1], wg.at[3], right),
        weights(7, wd.at[1, low], wd.at[3, low], right),
    ]
    on_left = [
        weights(8, wu.at[2], wu.at[3], left),
        weights(9, wd.at[2, high], wd.at[3, high], left),
    ]

    xin[...] = rms_rows(etok[...], egain[...])
    experts = lax.broadcasted_iota(jnp.int32, (n_ep, rows), 0)
    firsts = [ids_t[k : k + 1, :] == experts for k in range(2)]
    named = jnp.where(firsts[0] | firsts[1], 1.0, 0.0).astype(BF16)
    earlier = jnp.where(
        lax.broadcasted_iota(jnp.int32, (rows, rows), 0)
        < lax.broadcasted_iota(jnp.int32, (rows, rows), 1),
        1.0,
        0.0,
    ).astype(BF16)
    before = dot(named, earlier)
    targets_t = [
        ids_t[k : k + 1, :] * cap
        + jnp.sum(jnp.where(firsts[k], before, 0.0), axis=0, keepdims=True).astype(jnp.int32)
        for k in range(2)
    ]
    group = min(8, n_ep)

    @pl.loop(0, n_ep // group)
    def _(q):
        slots = lax.broadcasted_iota(jnp.int32, (group * cap, rows), 0) + q * group * cap
        place = jnp.where((slots == targets_t[0]) | (slots == targets_t[1]), 1.0, 0.0).astype(BF16)
        out_buf[pl.ds(q * group, group)] = (
            dot(place, xin[...]).astype(BF16).reshape(group, cap, width)
        )

    in_buf[n_ep - 1] = out_buf[ep]

    pl.semaphore_wait(barrier, n_ep - 1 + n_tp - 1)

    for a, b in zip(to_right, to_left):
        a.start()
        b.start()

    def token_copy(j):
        to = (ep + far_first(j, n_ep)) % n_ep
        return pltpu.make_async_remote_copy(
            src_ref=out_buf.at[to],
            dst_ref=in_buf.at[j],
            send_sem=tok_send.at[j],
            recv_sem=tok_recv.at[j],
            device_id={"ep": to},
            device_id_type=MESH,
        )

    @pl.loop(0, n_ep - 1)
    def _(j):
        token_copy(j).start()

    loads[3].wait()
    normed[tp] = rms_rows(mrows[...], mgain[...])

    acc[...] = jnp.zeros_like(acc)
    to_right[0].wait_recv()
    on_right[0].start()
    to_left[0].wait_recv()
    on_left[0].start()
    to_right[1].wait_recv()
    on_right[1].start()
    to_left[1].wait_recv()
    on_left[1].start()

    def spread(r):
        return pltpu.make_async_remote_copy(
            src_ref=normed.at[tp],
            dst_ref=normed.at[tp],
            send_sem=ag_send.at[r],
            recv_sem=ag_recv.at[r],
            device_id={"tp": (tp + r) % n_tp},
            device_id_type=MESH,
        )

    for r in (2, 1, 3):
        spread(r).start()

    for i in range(3):
        loads[i].wait()

    @pl.loop(0, n_ep - 1)
    def _(j):
        token_copy(j).wait_recv()

    tiles = 2
    per_tile = n_ep // tiles
    tile_rows = per_tile * cap
    step = min(512, width)

    def serve(s, m, last):
        x = in_buf[pl.ds(m * per_tile, per_tile)].reshape(tile_rows, width)
        g = dot(x, wg[s])
        u = dot(x, wu[s])
        hidden = (g / (1.0 + jnp.exp(-g)) * u).astype(BF16)
        for c in range(0, width, step):
            part = dot(hidden, wd[s, :, c : c + step]).astype(BF16).astype(F32)
            total = acc[m, :, c : c + step] + part
            if last:
                res_buf[pl.ds(m * per_tile, per_tile), :, c : c + step] = total.astype(BF16).reshape(
                    per_tile, cap, step
                )
            else:
                acc[m, :, c : c + step] = total

    def serve_all(s):
        @pl.loop(0, tiles)
        def _(m):
            serve(s, m, False)

    serve_all(0)
    to_right[2].wait_recv()
    serve_all(1)
    to_left[2].wait_recv()
    serve_all(2)
    for copy in (*on_right, *on_left):
        copy.wait_recv()

    def result_copy(j):
        to = (ep + n_ep - far_first(j, n_ep)) % n_ep
        return pltpu.make_async_remote_copy(
            src_ref=res_buf.at[j],
            dst_ref=ret_buf.at[ep],
            send_sem=ret_send.at[j],
            recv_sem=ret_recv.at[j],
            device_id={"ep": to},
            device_id_type=MESH,
        )

    @pl.loop(0, tiles)
    def _(m):
        serve(3, m, True)

        @pl.loop(m * per_tile, jnp.minimum((m + 1) * per_tile, n_ep - 1))
        def _(j):
            result_copy(j).start()

    ret_buf[ep] = res_buf[n_ep - 1]

    for i in range(4, 7):
        loads[i].wait()
    ext[0] = jnp.zeros((rows, ext.shape[2]), BF16)
    ext[tp + 1] = dot(normed[tp], inw_v[...]).astype(BF16)
    for r in (1, 3, 2):
        spread(r).wait_recv()
        src = (tp + n_tp - r) % n_tp
        ext[src + 1] = dot(normed[src], inw_v[...]).astype(BF16)
    edge = pl.ds(rows - WINDOW_MAX, WINDOW_MAX)
    halo = pltpu.make_async_remote_copy(
        src_ref=ext.at[n_tp, edge],
        dst_ref=ext.at[n_tp + 1, pl.ds(0, WINDOW_MAX)],
        send_sem=halo_send,
        recv_sem=halo_recv,
        device_id={"ep": (ep + 1) % n_ep},
        device_id_type=MESH,
    )
    halo.start()
    window = jnp.left_shift(jnp.int32(2), tp)
    lag = lax.broadcasted_iota(jnp.int32, (rows, rows), 0) - lax.broadcasted_iota(
        jnp.int32, (rows, rows), 1
    )
    band = jnp.where((lag >= 0) & (lag < window), 1.0, 0.0).astype(BF16)
    band_before = jnp.where(lag + rows < window, 1.0, 0.0).astype(BF16)
    place_in = lax.broadcasted_iota(jnp.int32, (rows, 1), 0) + 1
    halo.wait_recv()
    ext[0, edge, :] = jnp.where(ep == 0, 0.0, ext[n_tp + 1, 0:WINDOW_MAX, :].astype(F32)).astype(BF16)

    def sums(r):
        to = (tp + r) % n_tp
        return pltpu.make_async_remote_copy(
            src_ref=part_buf.at[to],
            dst_ref=part_in.at[r - 1],
            send_sem=rs_send.at[r],
            recv_sem=rs_recv.at[r],
            device_id={"tp": to},
            device_id_type=MESH,
        )

    for r in (2, 1, 3, 0):
        m = (tp + r) % n_tp
        here = ext[m + 1]
        total = dot(band, here) + dot(band_before, ext[m])
        counts = jnp.minimum(place_in + (ep * n_tp + m) * rows, window).astype(F32)
        pooled = (total / counts - here.astype(F32)).astype(BF16)
        grouped = (dot(pooled, gw_v[...]) * scale[...].astype(F32)).astype(BF16)
        for c in range(0, width, step):
            part_buf[m, :, c : c + step] = dot(grouped, ow_v[:, c : c + step]).astype(BF16)
        if r:
            sums(r).start()

    for r in (1, 3, 2):
        sums(r).wait_recv()
    total = part_buf[tp].astype(F32)
    for r in range(n_tp - 1):
        total = total + part_in[r].astype(F32)
    mixed_v[...] = total.astype(BF16)
    mixed_store = pltpu.make_async_copy(mixed_v, mixed_out, out_sem.at[0])
    mixed_store.start()

    lanes = lax.broadcasted_iota(jnp.int32, (rows, n_ep), 1)
    mine = [ids[:, k : k + 1] == lanes for k in range(2)]
    named_rows = jnp.where(mine[0] | mine[1], 1.0, 0.0).astype(BF16)
    later = jnp.where(lag > 0, 1.0, 0.0).astype(BF16)
    before_rows = dot(later, named_rows)
    slots = lax.broadcasted_iota(jnp.int32, (rows, n_slots), 1)
    picks = []
    for k in range(2):
        target = ids[:, k : k + 1] * cap + jnp.sum(
            jnp.where(mine[k], before_rows, 0.0), axis=1, keepdims=True
        ).astype(jnp.int32)
        picks.append(jnp.where(slots == target, 1.0, 0.0).astype(BF16))
    weight = shares[...]
    weight = weight / jnp.sum(weight, axis=1, keepdims=True)

    @pl.loop(0, n_ep - 1)
    def _(j):
        result_copy(j).wait_recv()

    for c in range(0, width, step):
        back = ret_buf[:, :, c : c + step].reshape(n_slots, step)
        mix = dot(picks[0], back) * weight[:, 0:1] + dot(picks[1], back) * weight[:, 1:2]
        expert_v[:, c : c + step] = mix.astype(BF16)
    expert_store = pltpu.make_async_copy(expert_v, expert_out, out_sem.at[1])
    expert_store.start()

    for copy in (*to_right, *to_left, *on_right, *on_left):
        copy.wait_send()

    @pl.loop(0, n_ep - 1)
    def _(j):
        token_copy(j).wait_send()
        result_copy(j).wait_send()

    for r in range(1, n_tp):
        spread(r).wait_send()
        sums(r).wait_send()
    halo.wait_send()
    mixed_store.wait()
    expert_store.wait()


def solution(mesh):
    n_ep, n_tp = mesh.shape["ep"], mesh.shape["tp"]

    def local(
        mixer_tokens, mixer_gain, in_weight, group_weight, channel_scale, out_weight,
        expert_tokens, expert_gain, route_ids, route_weights, gate_weight, up_weight, down_weight,
    ):
        rows, width = expert_tokens.shape
        cap = 4 * rows // n_ep
        gw = in_weight.shape[1]
        ff = gate_weight.shape[2]
        vmem = pl.BlockSpec(memory_space=pltpu.VMEM)
        hbm = pl.BlockSpec(memory_space=pl.ANY)
        slots = n_ep * cap
        V = pltpu.VMEM
        dma = pltpu.SemaphoreType.DMA
        out = jax.ShapeDtypeStruct((rows, width), BF16)
        return pl.pallas_call(
            functools.partial(kernel, n_ep, n_tp, cap),
            out_shape=(out, out),
            in_specs=[hbm, vmem, hbm, hbm, vmem, hbm, vmem, vmem, vmem, vmem, vmem, hbm, hbm, hbm],
            out_specs=(hbm, hbm),
            scratch_shapes=[
                V((rows, width), BF16),
                V((n_ep, cap, width), BF16),
                V((n_ep, cap, width), BF16),
                V((n_ep, cap, width), BF16),
                V((n_ep, cap, width), BF16),
                V((2, slots // 2, width), F32),
                V((n_tp, width, ff), BF16),
                V((n_tp, width, ff), BF16),
                V((n_tp, ff, width), BF16),
                V((rows, width), BF16),
                V((n_tp, rows, width), BF16),
                V((width, gw), BF16),
                V((gw, gw), BF16),
                V((gw, width), BF16),
                V((n_tp + 2, rows, gw), BF16),
                V((n_tp, rows, width), BF16),
                V((n_tp - 1, rows, width), BF16),
                V((rows, width), BF16),
                V((rows, width), BF16),
                dma((7,)),
                dma((n_ep - 1,)),
                dma((n_ep - 1,)),
                dma((n_ep - 1,)),
                dma((n_ep - 1,)),
                dma((10,)),
                dma((10,)),
                dma((n_tp,)),
                dma((n_tp,)),
                dma,
                dma,
                dma((n_tp,)),
                dma((n_tp,)),
                dma((2,)),
            ],
            compiler_params=pltpu.CompilerParams(
                collective_id=0, has_side_effects=True, vmem_limit_bytes=58 * 1024 * 1024
            ),
        )(
            mixer_tokens, mixer_gain[None], in_weight, group_weight, channel_scale[None], out_weight,
            expert_tokens, expert_gain[None], route_ids, route_ids.T, route_weights,
            gate_weight, up_weight, down_weight,
        )

    block = P(("grp", "ep", "tp"), None)
    placed = (
        block, P(), P(None, "tp"), P("tp", None, None), P("tp"), P("tp", None),
        block, P(), block, block, P("ep", None, "tp"), P("ep", None, "tp"), P("ep", "tp", None),
    )
    return jax.shard_map(
        local, mesh=mesh, in_specs=placed, out_specs=(block, block), check_vma=False
    )
```

time: 459 us -> 252 us (0.55)
  the two profiles are of different devices: /device:TPU:45 before, /device:TPU:40 now
where the time goes in v1:
time: 252 us; the launch traced here: 251 us
  Pallas kernels  240 us (95%)
  local copies, waits for them, and re-layouts  10.4 us (4%)
    pallas_call x1, Pallas kernels, local(): pl.pallas_call(functools.partial(kernel, n_ep, n_tp, cap), out_shape=(out...  240 us
    unnamed x4, local copies, waits for them, and re-layouts  6.59 us

profile of v1, /device:TPU:40, one launch (start us, length us, event | category | flops | bytes accessed | tf_op | source)
XLA Modules:
  0.0 251.4 jit_solution(8376407364687734578)
XLA Ops:
  0.6 1.3 broadcast_in_dim.10.scale
  1.9 1.3 broadcast_in_dim.9.mgain
  3.2 1.3 broadcast_in_dim.11.egain
  4.5 1.4 copy.16.shares
  5.9 1.4 copy.15.ids
  7.3 240.3 %shard_map.140 = (bf16[128,2048]{1,0:T(8,128)(2,1)}, bf16[128,2048]{1,0:T(8,128)(2,1)}) custom-call(bf16[128,2048]{1,0:T(8,128)(2,1)} %mtok.1, bf16[1,2048]{1,0:T(2,128)(2,1)} %broadcast_in_dim.9.mgain, bf16[2048,512]{1,0:T(8,128)(2,1)} %inw.1, bf16[1,512,512]{2,1,0:T(8,128)(2,1)} %gw.1, bf16[1,512]{1,0:T(2,128)(2,1)} %broadcast_in_dim.10.scale, ...), custom_call_target="tpu_custom_call" | custom-call | tf_op jit(solution)/shard_map/pallas_call | solution.py:362
  247.6 1.9 copy.19
  249.5 1.9 copy.20

commit v2 on v1

--- a/solution.py
+++ b/solution.py
@@ -20,7 +20,7 @@
 def rms_rows(rows, gain):
     values = rows.astype(F32)
     scaled = values * lax.rsqrt(jnp.mean(values * values, axis=-1, keepdims=True) + 1e-06)
-    return (scaled * gain.astype(F32)).astype(BF16)
+    return (scaled * gain.astype(F32)[None]).astype(BF16)
 
 
 def far_first(j, n):
@@ -29,16 +29,17 @@
 
 def kernel(
     n_ep, n_tp, cap,
-    mtok, mgain, inw, gw, scale, ow, etok, egain, ids, ids_t, shares, gate, up, down,
+    mtok, mgain_h, inw, gw, scale_h, ow, etok_h, egain_h, ids_h, shares_h, gate, up, down,
     mixed_out, expert_out,
+    etok, egain, mgain, scale, ids_t, shares_t,
     xin, out_buf, in_buf, res_buf, ret_buf, acc, wg, wu, wd,
-    mrows, normed, inw_v, gw_v, ow_v, ext, part_buf, part_in, mixed_v, expert_v,
+    mrows, normed, tail, edge_out, edge_in, inw_v, gw_v, ow_v, ext, part_buf, part_in,
     load_sem, tok_send, tok_recv, ret_send, ret_recv, w_send, w_recv,
-    ag_send, ag_recv, halo_send, halo_recv, rs_send, rs_recv, out_sem,
+    ag_send, ag_recv, tail_send, tail_recv, halo_send, halo_recv, rs_send, rs_recv,
 ):
     ep = lax.axis_index("ep")
     tp = lax.axis_index("tp")
-    rows, width = etok.shape
+    rows, width = mtok.shape
     n_slots = n_ep * cap
     half = n_ep // 2
     right, left = (tp + 1) % n_tp, (tp + n_tp - 1) % n_tp
@@ -61,11 +62,17 @@
         pltpu.make_async_copy(src, dst, load_sem.at[i])
         for i, (src, dst) in enumerate(
             [
+                (etok_h, etok),
+                (egain_h, egain),
+                (ids_h, ids_t),
+                (shares_h, shares_t),
+                (mgain_h, mgain),
+                (scale_h, scale),
+                (mtok, mrows),
+                (inw, inw_v),
                 (gate.at[0], wg.at[0]),
                 (up.at[0], wu.at[0]),
                 (down.at[0], wd.at[0]),
-                (mtok, mrows),
-                (inw, inw_v),
                 (gw.at[0], gw_v),
                 (ow, ow_v),
             ]
@@ -73,6 +80,8 @@
     ]
     for load in loads:
         load.start()
+    for i in range(3):
+        loads[i].wait()
 
     def weights(i, src, dst, to):
         return pltpu.make_async_remote_copy(
@@ -153,8 +162,44 @@
     def _(j):
         token_copy(j).start()
 
-    loads[3].wait()
+    loads[4].wait()
+    loads[6].wait()
     normed[tp] = rms_rows(mrows[...], mgain[...])
+
+    edge = pl.ds(rows - WINDOW_MAX, WINDOW_MAX)
+
+    def tail_copy(r):
+        return pltpu.make_async_remote_copy(
+            src_ref=normed.at[n_tp - 1, edge],
+            dst_ref=tail,
+            send_sem=tail_send.at[r],
+            recv_sem=tail_recv,
+            device_id={"tp": (tp + r) % n_tp},
+            device_id_type=MESH,
+        )
+
+    loads[7].wait()
+
+    @pl.when(tp == n_tp - 1)
+    def _():
+        for r in (2, 1, 3):
+            tail_copy(r).start()
+        tail[...] = normed[n_tp - 1, edge]
+
+    @pl.when(tp != n_tp - 1)
+    def _():
+        tail_copy(0).wait_recv()
+
+    edge_out[...] = dot(tail[...], inw_v[...]).astype(BF16)
+    halo = pltpu.make_async_remote_copy(
+        src_ref=edge_out,
+        dst_ref=edge_in,
+        send_sem=halo_send,
+        recv_sem=halo_recv,
+        device_id={"ep": (ep + 1) % n_ep},
+        device_id_type=MESH,
+    )
+    halo.start()
 
     acc[...] = jnp.zeros_like(acc)
     to_right[0].wait_recv()
@@ -179,7 +224,7 @@
     for r in (2, 1, 3):
         spread(r).start()
 
-    for i in range(3):
+    for i in range(8, 11):
         loads[i].wait()
 
     @pl.loop(0, n_ep - 1)
@@ -240,7 +285,7 @@
 
     ret_buf[ep] = res_buf[n_ep - 1]
 
-    for i in range(4, 7):
+    for i in (3, 5, 11, 12):
         loads[i].wait()
     ext[0] = jnp.zeros((rows, ext.shape[2]), BF16)
     ext[tp + 1] = dot(normed[tp], inw_v[...]).astype(BF16)
@@ -248,16 +293,6 @@
         spread(r).wait_recv()
         src = (tp + n_tp - r) % n_tp
         ext[src + 1] = dot(normed[src], inw_v[...]).astype(BF16)
-    edge = pl.ds(rows - WINDOW_MAX, WINDOW_MAX)
-    halo = pltpu.make_async_remote_copy(
-        src_ref=ext.at[n_tp, edge],
-        dst_ref=ext.at[n_tp + 1, pl.ds(0, WINDOW_MAX)],
-        send_sem=halo_send,
-        recv_sem=halo_recv,
-        device_id={"ep": (ep + 1) % n_ep},
-        device_id_type=MESH,
-    )
-    halo.start()
     window = jnp.left_shift(jnp.int32(2), tp)
     lag = lax.broadcasted_iota(jnp.int32, (rows, rows), 0) - lax.broadcasted_iota(
         jnp.int32, (rows, rows), 1
@@ -266,7 +301,7 @@
     band_before = jnp.where(lag + rows < window, 1.0, 0.0).astype(BF16)
     place_in = lax.broadcasted_iota(jnp.int32, (rows, 1), 0) + 1
     halo.wait_recv()
-    ext[0, edge, :] = jnp.where(ep == 0, 0.0, ext[n_tp + 1, 0:WINDOW_MAX, :].astype(F32)).astype(BF16)
+    ext[0, edge, :] = jnp.where(ep == 0, 0.0, edge_in[...].astype(F32)).astype(BF16)
 
     def sums(r):
         to = (tp + r) % n_tp
@@ -285,7 +320,7 @@
         total = dot(band, here) + dot(band_before, ext[m])
         counts = jnp.minimum(place_in + (ep * n_tp + m) * rows, window).astype(F32)
         pooled = (total / counts - here.astype(F32)).astype(BF16)
-        grouped = (dot(pooled, gw_v[...]) * scale[...].astype(F32)).astype(BF16)
+        grouped = (dot(pooled, gw_v[...]) * scale[...].astype(F32)[None]).astype(BF16)
         for c in range(0, width, step):
             part_buf[m, :, c : c + step] = dot(grouped, ow_v[:, c : c + step]).astype(BF16)
         if r:
@@ -296,10 +331,10 @@
     total = part_buf[tp].astype(F32)
     for r in range(n_tp - 1):
         total = total + part_in[r].astype(F32)
-    mixed_v[...] = total.astype(BF16)
-    mixed_store = pltpu.make_async_copy(mixed_v, mixed_out, out_sem.at[0])
-    mixed_store.start()
-
+    mixed_out[...] = total.astype(BF16)
+
+    ids = jnp.transpose(ids_t[...])
+    shares = jnp.transpose(shares_t[...])
     lanes = lax.broadcasted_iota(jnp.int32, (rows, n_ep), 1)
     mine = [ids[:, k : k + 1] == lanes for k in range(2)]
     named_rows = jnp.where(mine[0] | mine[1], 1.0, 0.0).astype(BF16)
@@ -312,8 +347,7 @@
             jnp.where(mine[k], before_rows, 0.0), axis=1, keepdims=True
         ).astype(jnp.int32)
         picks.append(jnp.where(slots == target, 1.0, 0.0).astype(BF16))
-    weight = shares[...]
-    weight = weight / jnp.sum(weight, axis=1, keepdims=True)
+    weight = shares / jnp.sum(shares, axis=1, keepdims=True)
 
     @pl.loop(0, n_ep - 1)
     def _(j):
@@ -322,9 +356,7 @@
     for c in range(0, width, step):
         back = ret_buf[:, :, c : c + step].reshape(n_slots, step)
         mix = dot(picks[0], back) * weight[:, 0:1] + dot(picks[1], back) * weight[:, 1:2]
-        expert_v[:, c : c + step] = mix.astype(BF16)
-    expert_store = pltpu.make_async_copy(expert_v, expert_out, out_sem.at[1])
-    expert_store.start()
+        expert_out[:, c : c + step] = mix.astype(BF16)
 
     for copy in (*to_right, *to_left, *on_right, *on_left):
         copy.wait_send()
@@ -338,8 +370,11 @@
         spread(r).wait_send()
         sums(r).wait_send()
     halo.wait_send()
-    mixed_store.wait()
-    expert_store.wait()
+
+    @pl.when(tp == n_tp - 1)
+    def _():
+        for r in range(1, n_tp):
+            tail_copy(r).wait_send()
 
 
 def solution(mesh):
@@ -362,9 +397,15 @@
         return pl.pallas_call(
             functools.partial(kernel, n_ep, n_tp, cap),
             out_shape=(out, out),
-            in_specs=[hbm, vmem, hbm, hbm, vmem, hbm, vmem, vmem, vmem, vmem, vmem, hbm, hbm, hbm],
-            out_specs=(hbm, hbm),
+            in_specs=[hbm] * 13,
+            out_specs=(vmem, vmem),
             scratch_shapes=[
+                V((rows, width), BF16),
+                V((width,), BF16),
+                V((width,), BF16),
+                V((gw,), BF16),
+                V((2, rows), jnp.int32),
+                V((2, rows), F32),
                 V((rows, width), BF16),
                 V((n_ep, cap, width), BF16),
                 V((n_ep, cap, width), BF16),
@@ -376,15 +417,16 @@
                 V((n_tp, ff, width), BF16),
                 V((rows, width), BF16),
                 V((n_tp, rows, width), BF16),
+                V((WINDOW_MAX, width), BF16),
+                V((WINDOW_MAX, gw), BF16),
+                V((WINDOW_MAX, gw), BF16),
                 V((width, gw), BF16),
                 V((gw, gw), BF16),
                 V((gw, width), BF16),
-                V((n_tp + 2, rows, gw), BF16),
+                V((n_tp + 1, rows, gw), BF16),
                 V((n_tp, rows, width), BF16),
                 V((n_tp - 1, rows, width), BF16),
-                V((rows, width), BF16),
-                V((rows, width), BF16),
-                dma((7,)),
+                dma((13,)),
                 dma((n_ep - 1,)),
                 dma((n_ep - 1,)),
                 dma((n_ep - 1,)),
@@ -393,19 +435,25 @@
                 dma((10,)),
                 dma((n_tp,)),
                 dma((n_tp,)),
+                dma((n_tp,)),
+                dma,
                 dma,
                 dma,
                 dma((n_tp,)),
                 dma((n_tp,)),
-                dma((2,)),
             ],
             compiler_params=pltpu.CompilerParams(
-                collective_id=0, has_side_effects=True, vmem_limit_bytes=58 * 1024 * 1024
+                collective_id=0, has_side_effects=True, vmem_limit_bytes=52 * 1024 * 1024
             ),
         )(
-            mixer_tokens, mixer_gain[None], in_weight, group_weight, channel_scale[None], out_weight,
-            expert_tokens, expert_gain[None], route_ids, route_ids.T, route_weights,
-            gate_weight, up_weight, down_weight,
+            *(
+                pltpu.with_memory_space_constraint(a, pltpu.HBM)
+                for a in (
+                    mixer_tokens, mixer_gain, in_weight, group_weight, channel_scale, out_weight,
+                    expert_tokens, expert_gain, route_ids.T, route_weights.T,
+                    gate_weight, up_weight, down_weight,
+                )
+            )
         )
 
     block = P(("grp", "ep", "tp"), None)

time: 252 us -> 230 us (0.913)
  the two profiles are of different devices: /device:TPU:40 before, /device:TPU:45 now
where the time goes in v2:
time: 230 us; the launch traced here: 227 us
  Pallas kernels  225 us (98%)
    pallas_call x1, Pallas kernels, local(): pl.pallas_call(functools.partial(kernel, n_ep, n_tp, cap), out_shape=(out...  225 us

profile of v2, /device:TPU:45, one launch (start us, length us, event | category | flops | bytes accessed | tf_op | source)
XLA Modules:
  0.0 227.3 jit_solution(8343229954360455463)
XLA Ops:
  0.6 225.1 %shard_map.140 = (bf16[128,2048]{1,0:T(8,128)(2,1)S(1)}, bf16[128,2048]{1,0:T(8,128)(2,1)S(1)}) custom-call(bf16[128,2048]{1,0:T(8,128)(2,1)} %mtok.1, bf16[2048]{0:T(1024)(128)(2,1)} %mgain_h.1, bf16[2048,512]{1,0:T(8,128)(2,1)} %inw.1, bf16[1,512,512]{2,1,0:T(8,128)(2,1)} %gw.1, bf16[512]{0:T(512)(128)(2,1)} %scale_h.1, bf16[512,2048]{1,0:T(8,128)(2,1)} %ow.1, ...), custom_call_target="tpu_custom_call" | custom-call | tf_op jit(solution)/shard_map/pallas_call | solution.py:397
  225.7 0.8 copy.17
  226.5 0.8 copy.18

commit v3 on v2

--- a/solution.py
+++ b/solution.py
@@ -32,18 +32,18 @@
     mtok, mgain_h, inw, gw, scale_h, ow, etok_h, egain_h, ids_h, shares_h, gate, up, down,
     mixed_out, expert_out,
     etok, egain, mgain, scale, ids_t, shares_t,
-    xin, out_buf, in_buf, res_buf, ret_buf, acc, wg, wu, wd,
+    xin, out_buf, in_buf, peer_buf, res_buf, ret_buf, acc, part_out, part_back, wg, wu, wd,
     mrows, normed, tail, edge_out, edge_in, inw_v, gw_v, ow_v, ext, part_buf, part_in,
-    load_sem, tok_send, tok_recv, ret_send, ret_recv, w_send, w_recv,
+    load_sem, tok_send, tok_recv, swap_send, swap_recv, back_send, back_recv,
+    ret_send, ret_recv, w_send, w_recv,
     ag_send, ag_recv, tail_send, tail_recv, halo_send, halo_recv, rs_send, rs_recv,
 ):
     ep = lax.axis_index("ep")
     tp = lax.axis_index("tp")
     rows, width = mtok.shape
     n_slots = n_ep * cap
-    half = n_ep // 2
-    right, left = (tp + 1) % n_tp, (tp + n_tp - 1) % n_tp
-    depth = down.shape[1]
+    n_z = n_ep // 2
+    z, core = ep // 2, ep % 2
 
     barrier = pltpu.get_barrier_semaphore()
 
@@ -83,34 +83,20 @@
     for i in range(3):
         loads[i].wait()
 
-    def weights(i, src, dst, to):
+    def weights(i, src, dst):
         return pltpu.make_async_remote_copy(
             src_ref=src,
             dst_ref=dst,
             send_sem=w_send.at[i],
             recv_sem=w_recv.at[i],
-            device_id={"tp": to},
-            device_id_type=MESH,
-        )
-
-    low, high = pl.ds(0, depth // 2), pl.ds(depth // 2, depth // 2)
-    to_right = [
-        weights(0, gate.at[0], wg.at[1], right),
-        weights(1, down.at[0], wd.at[1], right),
-        weights(2, up.at[0], wu.at[1], right),
-    ]
-    to_left = [
-        weights(3, up.at[0], wu.at[2], left),
-        weights(4, down.at[0], wd.at[2], left),
-        weights(5, gate.at[0], wg.at[2], left),
-    ]
-    on_right = [
-        weights(6, wg.at[1], wg.at[3], right),
-        weights(7, wd.at[1, low], wd.at[3, low], right),
-    ]
-    on_left = [
-        weights(8, wu.at[2], wu.at[3], left),
-        weights(9, wd.at[2, high], wd.at[3, high], left),
+            device_id={"tp": tp + 1 - 2 * (tp % 2)},
+            device_id_type=MESH,
+        )
+
+    shard_copies = [
+        weights(0, gate.at[0], wg.at[1]),
+        weights(1, up.at[0], wu.at[1]),
+        weights(2, down.at[0], wd.at[1]),
     ]
 
     xin[...] = rms_rows(etok[...], egain[...])
@@ -139,28 +125,49 @@
             dot(place, xin[...]).astype(BF16).reshape(group, cap, width)
         )
 
-    in_buf[n_ep - 1] = out_buf[ep]
+    last = n_z - 1
+    in_buf[2 * last + core] = out_buf[ep]
 
     pl.semaphore_wait(barrier, n_ep - 1 + n_tp - 1)
 
-    for a, b in zip(to_right, to_left):
-        a.start()
-        b.start()
-
-    def token_copy(j):
-        to = (ep + far_first(j, n_ep)) % n_ep
+    for copy in shard_copies:
+        copy.start()
+
+    def token_copy(o, k):
+        to = 2 * ((z + far_first(o, n_z)) % n_z) + k
         return pltpu.make_async_remote_copy(
             src_ref=out_buf.at[to],
-            dst_ref=in_buf.at[j],
-            send_sem=tok_send.at[j],
-            recv_sem=tok_recv.at[j],
+            dst_ref=in_buf.at[2 * o + core],
+            send_sem=tok_send.at[2 * o + k],
+            recv_sem=tok_recv.at[2 * o + core],
             device_id={"ep": to},
             device_id_type=MESH,
         )
 
-    @pl.loop(0, n_ep - 1)
-    def _(j):
-        token_copy(j).start()
+    def token_arrival(o, k):
+        return pltpu.make_async_remote_copy(
+            src_ref=in_buf.at[2 * o + k],
+            dst_ref=in_buf.at[2 * o + k],
+            send_sem=tok_send.at[2 * o + k],
+            recv_sem=tok_recv.at[2 * o + k],
+            device_id={"ep": 2 * z + 1 - core},
+            device_id_type=MESH,
+        )
+
+    sibling = pltpu.make_async_remote_copy(
+        src_ref=out_buf.at[2 * z + 1 - core],
+        dst_ref=in_buf.at[2 * last + core],
+        send_sem=tok_send.at[2 * last + 1 - core],
+        recv_sem=tok_recv.at[2 * last + core],
+        device_id={"ep": 2 * z + 1 - core},
+        device_id_type=MESH,
+    )
+    sibling.start()
+
+    @pl.loop(0, last)
+    def _(o):
+        for k in range(2):
+            token_copy(o, k).start()
 
     loads[4].wait()
     loads[6].wait()
@@ -201,16 +208,6 @@
     )
     halo.start()
 
-    acc[...] = jnp.zeros_like(acc)
-    to_right[0].wait_recv()
-    on_right[0].start()
-    to_left[0].wait_recv()
-    on_left[0].start()
-    to_right[1].wait_recv()
-    on_right[1].start()
-    to_left[1].wait_recv()
-    on_left[1].start()
-
     def spread(r):
         return pltpu.make_async_remote_copy(
             src_ref=normed.at[tp],
@@ -221,69 +218,130 @@
             device_id_type=MESH,
         )
 
+    groups = 4
+    chips = n_z // groups
+    per = 2 * chips
+    half_rows = per * cap
+    step = min(512, width)
+    across = n_tp - 1 - tp
+
+    def swap(o):
+        return pltpu.make_async_remote_copy(
+            src_ref=in_buf.at[pl.ds(2 * o, 2)],
+            dst_ref=peer_buf.at[pl.ds(2 * o, 2)],
+            send_sem=swap_send.at[o],
+            recv_sem=swap_recv.at[o],
+            device_id={"tp": across},
+            device_id_type=MESH,
+        )
+
+    def pass_on(first, end):
+        @pl.loop(first, min(end, last))
+        def _(o):
+            for k in range(2):
+                token_arrival(o, k).wait_recv()
+            swap(o).start()
+
+        if end == n_z:
+            token_arrival(last, 1 - core).wait_recv()
+            swap(last).start()
+
+    def partial_copy(g):
+        return pltpu.make_async_remote_copy(
+            src_ref=part_out.at[g],
+            dst_ref=part_back.at[g],
+            send_sem=back_send.at[g],
+            recv_sem=back_recv.at[g],
+            device_id={"tp": across},
+            device_id_type=MESH,
+        )
+
+    def serve(g):
+        @pl.loop(g * chips, (g + 1) * chips)
+        def _(o):
+            swap(o).wait_recv()
+
+        mine = pl.ds(g * per, per)
+        x = jnp.concatenate(
+            [
+                peer_buf[mine].reshape(half_rows, width),
+                in_buf[mine].reshape(half_rows, width),
+            ],
+            axis=0,
+        )
+        hidden = []
+        for s in range(2):
+            gate_in = dot(x, wg[s])
+            hidden.append((gate_in / (1.0 + jnp.exp(-gate_in)) * dot(x, wu[s])).astype(BF16))
+        for c in range(0, width, step):
+            total = dot(hidden[0], wd[0, :, c : c + step]).astype(BF16).astype(F32)
+            total = total + dot(hidden[1], wd[1, :, c : c + step]).astype(BF16).astype(F32)
+            part_out[g, :, c : c + step] = total[:half_rows].astype(BF16)
+            acc[g, :, c : c + step] = total[half_rows:]
+        partial_copy(g).start()
+
+    def result_copy(o, k):
+        to = 2 * ((z + n_z - far_first(o, n_z)) % n_z) + k
+        return pltpu.make_async_remote_copy(
+            src_ref=res_buf.at[2 * o + k],
+            dst_ref=ret_buf.at[ep],
+            send_sem=ret_send.at[2 * o + k],
+            recv_sem=ret_recv.at[2 * o + core],
+            device_id={"ep": to},
+            device_id_type=MESH,
+        )
+
+    def result_arrival(o, k):
+        sender = 2 * ((z + far_first(o, n_z)) % n_z) + k
+        return pltpu.make_async_remote_copy(
+            src_ref=res_buf.at[2 * o + k],
+            dst_ref=ret_buf.at[sender],
+            send_sem=ret_send.at[2 * o + k],
+            recv_sem=ret_recv.at[2 * o + k],
+            device_id={"ep": 2 * z + 1 - core},
+            device_id_type=MESH,
+        )
+
+    sibling_back = pltpu.make_async_remote_copy(
+        src_ref=res_buf.at[2 * last + 1 - core],
+        dst_ref=ret_buf.at[ep],
+        send_sem=ret_send.at[2 * last + 1 - core],
+        recv_sem=ret_recv.at[2 * last + core],
+        device_id={"ep": 2 * z + 1 - core},
+        device_id_type=MESH,
+    )
+
+    def answer(g):
+        partial_copy(g).wait_recv()
+        res_buf[pl.ds(g * per, per)] = (
+            (acc[g] + part_back[g].astype(F32)).astype(BF16).reshape(per, cap, width)
+        )
+
+        @pl.loop(g * chips, min((g + 1) * chips, last))
+        def _(o):
+            for k in range(2):
+                result_copy(o, k).start()
+
+        if g == groups - 1:
+            sibling_back.start()
+            ret_buf[ep] = res_buf[2 * last + core]
+
+    pass_on(0, 3 * chips)
+    for i in range(8, 11):
+        loads[i].wait()
+    for copy in shard_copies:
+        copy.wait_recv()
+    for g in range(groups - 1):
+        serve(g)
+    middle = 3 * chips + chips // 2
+    pass_on(3 * chips, middle)
+    answer(0)
+    pass_on(middle, n_z)
+    serve(groups - 1)
     for r in (2, 1, 3):
         spread(r).start()
-
-    for i in range(8, 11):
-        loads[i].wait()
-
-    @pl.loop(0, n_ep - 1)
-    def _(j):
-        token_copy(j).wait_recv()
-
-    tiles = 2
-    per_tile = n_ep // tiles
-    tile_rows = per_tile * cap
-    step = min(512, width)
-
-    def serve(s, m, last):
-        x = in_buf[pl.ds(m * per_tile, per_tile)].reshape(tile_rows, width)
-        g = dot(x, wg[s])
-        u = dot(x, wu[s])
-        hidden = (g / (1.0 + jnp.exp(-g)) * u).astype(BF16)
-        for c in range(0, width, step):
-            part = dot(hidden, wd[s, :, c : c + step]).astype(BF16).astype(F32)
-            total = acc[m, :, c : c + step] + part
-            if last:
-                res_buf[pl.ds(m * per_tile, per_tile), :, c : c + step] = total.astype(BF16).reshape(
-                    per_tile, cap, step
-                )
-            else:
-                acc[m, :, c : c + step] = total
-
-    def serve_all(s):
-        @pl.loop(0, tiles)
-        def _(m):
-            serve(s, m, False)
-
-    serve_all(0)
-    to_right[2].wait_recv()
-    serve_all(1)
-    to_left[2].wait_recv()
-    serve_all(2)
-    for copy in (*on_right, *on_left):
-        copy.wait_recv()
-
-    def result_copy(j):
-        to = (ep + n_ep - far_first(j, n_ep)) % n_ep
-        return pltpu.make_async_remote_copy(
-            src_ref=res_buf.at[j],
-            dst_ref=ret_buf.at[ep],
-            send_sem=ret_send.at[j],
-            recv_sem=ret_recv.at[j],
-            device_id={"ep": to},
-            device_id_type=MESH,
-        )
-
-    @pl.loop(0, tiles)
-    def _(m):
-        serve(3, m, True)
-
-        @pl.loop(m * per_tile, jnp.minimum((m + 1) * per_tile, n_ep - 1))
-        def _(j):
-            result_copy(j).start()
-
-    ret_buf[ep] = res_buf[n_ep - 1]
+    for g in range(1, groups):
+        answer(g)
 
     for i in (3, 5, 11, 12):
         loads[i].wait()
@@ -349,22 +407,40 @@
         picks.append(jnp.where(slots == target, 1.0, 0.0).astype(BF16))
     weight = shares / jnp.sum(shares, axis=1, keepdims=True)
 
-    @pl.loop(0, n_ep - 1)
-    def _(j):
-        result_copy(j).wait_recv()
+    @pl.loop(0, last)
+    def _(o):
+        for k in range(2):
+            result_arrival(o, k).wait_recv()
+
+    pltpu.make_async_remote_copy(
+        src_ref=res_buf.at[2 * last + 1 - core],
+        dst_ref=ret_buf.at[2 * z + 1 - core],
+        send_sem=ret_send.at[2 * last + 1 - core],
+        recv_sem=ret_recv.at[2 * last + 1 - core],
+        device_id={"ep": 2 * z + 1 - core},
+        device_id_type=MESH,
+    ).wait_recv()
 
     for c in range(0, width, step):
         back = ret_buf[:, :, c : c + step].reshape(n_slots, step)
         mix = dot(picks[0], back) * weight[:, 0:1] + dot(picks[1], back) * weight[:, 1:2]
         expert_out[:, c : c + step] = mix.astype(BF16)
 
-    for copy in (*to_right, *to_left, *on_right, *on_left):
+    for copy in (*shard_copies, sibling, sibling_back):
         copy.wait_send()
 
-    @pl.loop(0, n_ep - 1)
-    def _(j):
-        token_copy(j).wait_send()
-        result_copy(j).wait_send()
+    @pl.loop(0, last)
+    def _(o):
+        for k in range(2):
+            token_copy(o, k).wait_send()
+            result_copy(o, k).wait_send()
+
+    @pl.loop(0, n_z)
+    def _(o):
+        swap(o).wait_send()
+
+    for g in range(groups):
+        partial_copy(g).wait_send()
 
     for r in range(1, n_tp):
         spread(r).wait_send()
@@ -411,10 +487,13 @@
                 V((n_ep, cap, width), BF16),
                 V((n_ep, cap, width), BF16),
                 V((n_ep, cap, width), BF16),
-                V((2, slots // 2, width), F32),
-                V((n_tp, width, ff), BF16),
-                V((n_tp, width, ff), BF16),
-                V((n_tp, ff, width), BF16),
+                V((n_ep, cap, width), BF16),
+                V((4, slots // 4, width), F32),
+                V((4, slots // 4, width), BF16),
+                V((4, slots // 4, width), BF16),
+                V((2, width, ff), BF16),
+                V((2, width, ff), BF16),
+                V((2, ff, width), BF16),
                 V((rows, width), BF16),
                 V((n_tp, rows, width), BF16),
                 V((WINDOW_MAX, width), BF16),
@@ -427,12 +506,16 @@
                 V((n_tp, rows, width), BF16),
                 V((n_tp - 1, rows, width), BF16),
                 dma((13,)),
-                dma((n_ep - 1,)),
-                dma((n_ep - 1,)),
-                dma((n_ep - 1,)),
-                dma((n_ep - 1,)),
-                dma((10,)),
-                dma((10,)),
+                dma((n_ep,)),
+                dma((n_ep,)),
+                dma((n_ep // 2,)),
+                dma((n_ep // 2,)),
+                dma((4,)),
+                dma((4,)),
+                dma((n_ep,)),
+                dma((n_ep,)),
+                dma((3,)),
+                dma((3,)),
                 dma((n_tp,)),
                 dma((n_tp,)),
                 dma((n_tp,)),

time: 230 us -> 256 us (1.11)
  Pallas kernels: 225 us -> 252 us
    pallas_call x1, Pallas kernels: 225 us -> 252 us  [local(): pl.pallas_call(functools.partial(kernel, n_ep, n_tp, cap), out_shape=(out...]
where the time goes in v3:
time: 256 us; the launch traced here: 254 us
  Pallas kernels  252 us (98%)
    pallas_call x1, Pallas kernels, local(): pl.pallas_call(functools.partial(kernel, n_ep, n_tp, cap), out_shape=(out...  252 us

profile of v3, /device:TPU:45, one launch (start us, length us, event | category | flops | bytes accessed | tf_op | source)
XLA Modules:
  0.0 253.9 jit_solution(4476604041826060123)
XLA Ops:
  0.6 251.6 %shard_map.140 = (bf16[128,2048]{1,0:T(8,128)(2,1)S(1)}, bf16[128,2048]{1,0:T(8,128)(2,1)S(1)}) custom-call(bf16[128,2048]{1,0:T(8,128)(2,1)} %mtok.1, bf16[2048]{0:T(1024)(128)(2,1)} %mgain_h.1, bf16[2048,512]{1,0:T(8,128)(2,1)} %inw.1, bf16[1,512,512]{2,1,0:T(8,128)(2,1)} %gw.1, bf16[512]{0:T(512)(128)(2,1)} %scale_h.1, bf16[512,2048]{1,0:T(8,128)(2,1)} %ow.1, ...), custom_call_target="tpu_custom_call" | custom-call | tf_op jit(solution)/shard_map/pallas_call | solution.py:473
  252.3 0.8 copy.17
  253.1 0.8 copy.18

commit v4 on v3

--- a/solution.py
+++ b/solution.py
@@ -23,8 +23,12 @@
     return (scaled * gain.astype(F32)[None]).astype(BF16)
 
 
-def far_first(j, n):
-    return n // 2 + (1 - 2 * (j % 2)) * ((j + 1) // 2)
+def offset(j, n):
+    if not isinstance(j, int):
+        pair, i = j // 4, j % 4
+        hops = (1 - i // 2) * (n // 2 - 1 - pair) + (i // 2) * (1 + pair)
+        return (n + (1 - 2 * (i % 2)) * hops) % n
+    return (n // 2, n // 4, 3 * n // 4, 0)[j - n + 4]
 
 
 def kernel(
@@ -42,6 +46,8 @@
     tp = lax.axis_index("tp")
     rows, width = mtok.shape
     n_slots = n_ep * cap
+    beside, across = tp + 1 - 2 * (tp % 2), n_tp - 1 - tp
+    opposite = n_tp - 1 - beside
     n_z = n_ep // 2
     z, core = ep // 2, ep % 2
 
@@ -89,7 +95,7 @@
             dst_ref=dst,
             send_sem=w_send.at[i],
             recv_sem=w_recv.at[i],
-            device_id={"tp": tp + 1 - 2 * (tp % 2)},
+            device_id={"tp": beside},
             device_id_type=MESH,
         )
 
@@ -128,13 +134,16 @@
     last = n_z - 1
     in_buf[2 * last + core] = out_buf[ep]
 
+    def each(first, end, work):
+        if first < n_z - 4:
+            pl.loop(first, min(end, n_z - 4))(work)
+        for o in range(max(first, n_z - 4), min(end, last)):
+            work(o)
+
     pl.semaphore_wait(barrier, n_ep - 1 + n_tp - 1)
 
-    for copy in shard_copies:
-        copy.start()
-
     def token_copy(o, k):
-        to = 2 * ((z + far_first(o, n_z)) % n_z) + k
+        to = 2 * ((z + offset(o, n_z)) % n_z) + k
         return pltpu.make_async_remote_copy(
             src_ref=out_buf.at[to],
             dst_ref=in_buf.at[2 * o + core],
@@ -164,10 +173,12 @@
     )
     sibling.start()
 
-    @pl.loop(0, last)
-    def _(o):
+    def send_tokens(o):
         for k in range(2):
             token_copy(o, k).start()
+
+    each(0, last, send_tokens)
+    shard_copies[0].start()
 
     loads[4].wait()
     loads[6].wait()
@@ -192,6 +203,131 @@
         for r in (2, 1, 3):
             tail_copy(r).start()
         tail[...] = normed[n_tp - 1, edge]
+
+    for copy in shard_copies[1:]:
+        copy.start()
+
+    def spread(i, src, to):
+        return pltpu.make_async_remote_copy(
+            src_ref=normed.at[src],
+            dst_ref=normed.at[src],
+            send_sem=ag_send.at[i],
+            recv_sem=ag_recv.at[i],
+            device_id={"tp": to},
+            device_id_type=MESH,
+        )
+
+    def spread_arrival(i, src):
+        return spread(i, src, across)
+
+    spreads = [spread(0, tp, across), spread(1, tp, beside), spread(2, across, beside)]
+    spreads[0].start()
+    spreads[1].start()
+
+    groups = 4
+    chips = n_z // groups
+    per = 2 * chips
+    half_rows = per * cap
+    step = min(512, width)
+
+    def swap(o):
+        return pltpu.make_async_remote_copy(
+            src_ref=in_buf.at[pl.ds(2 * o, 2)],
+            dst_ref=peer_buf.at[pl.ds(2 * o, 2)],
+            send_sem=swap_send.at[o],
+            recv_sem=swap_recv.at[o],
+            device_id={"tp": across},
+            device_id_type=MESH,
+        )
+
+    def pass_on(o):
+        for k in range(2):
+            token_arrival(o, k).wait_recv()
+        swap(o).start()
+
+    def partial_copy(g):
+        return pltpu.make_async_remote_copy(
+            src_ref=part_out.at[g],
+            dst_ref=part_back.at[g],
+            send_sem=back_send.at[g],
+            recv_sem=back_recv.at[g],
+            device_id={"tp": across},
+            device_id_type=MESH,
+        )
+
+    def serve(g):
+        @pl.loop(g * chips, (g + 1) * chips)
+        def _(o):
+            swap(o).wait_recv()
+
+        mine = pl.ds(g * per, per)
+        x = jnp.concatenate(
+            [
+                peer_buf[mine].reshape(half_rows, width),
+                in_buf[mine].reshape(half_rows, width),
+            ],
+            axis=0,
+        )
+        hidden = []
+        for s in range(2):
+            gate_in = dot(x, wg[s])
+            hidden.append((gate_in / (1.0 + jnp.exp(-gate_in)) * dot(x, wu[s])).astype(BF16))
+        for c in range(0, width, step):
+            total = dot(hidden[0], wd[0, :, c : c + step]).astype(BF16).astype(F32)
+            total = total + dot(hidden[1], wd[1, :, c : c + step]).astype(BF16).astype(F32)
+            part_out[g, :, c : c + step] = total[:half_rows].astype(BF16)
+            acc[g, :, c : c + step] = total[half_rows:]
+        partial_copy(g).start()
+
+    def result_copy(o, k):
+        to = 2 * ((z + n_z - offset(o, n_z)) % n_z) + k
+        return pltpu.make_async_remote_copy(
+            src_ref=res_buf.at[2 * o + k],
+            dst_ref=ret_buf.at[ep],
+            send_sem=ret_send.at[2 * o + k],
+            recv_sem=ret_recv.at[2 * o + core],
+            device_id={"ep": to},
+            device_id_type=MESH,
+        )
+
+    def result_arrival(o, k):
+        sender = 2 * ((z + offset(o, n_z)) % n_z) + k
+        return pltpu.make_async_remote_copy(
+            src_ref=res_buf.at[2 * o + k],
+            dst_ref=ret_buf.at[sender],
+            send_sem=ret_send.at[2 * o + k],
+            recv_sem=ret_recv.at[2 * o + k],
+            device_id={"ep": 2 * z + 1 - core},
+            device_id_type=MESH,
+        )
+
+    sibling_back = pltpu.make_async_remote_copy(
+        src_ref=res_buf.at[2 * last + 1 - core],
+        dst_ref=ret_buf.at[ep],
+        send_sem=ret_send.at[2 * last + 1 - core],
+        recv_sem=ret_recv.at[2 * last + core],
+        device_id={"ep": 2 * z + 1 - core},
+        device_id_type=MESH,
+    )
+
+    def answer(g):
+        partial_copy(g).wait_recv()
+        res_buf[pl.ds(g * per, per)] = (
+            (acc[g] + part_back[g].astype(F32)).astype(BF16).reshape(per, cap, width)
+        )
+
+        def send_results(o):
+            for k in range(2):
+                result_copy(o, k).start()
+
+        each(g * chips, (g + 1) * chips, send_results)
+        if g == groups - 1:
+            sibling_back.start()
+            ret_buf[ep] = res_buf[2 * last + core]
+
+    token_arrival(last, 1 - core).wait_recv()
+    swap(last).start()
+    each(0, 2 * chips, pass_on)
 
     @pl.when(tp != n_tp - 1)
     def _():
@@ -207,150 +343,31 @@
         device_id_type=MESH,
     )
     halo.start()
-
-    def spread(r):
-        return pltpu.make_async_remote_copy(
-            src_ref=normed.at[tp],
-            dst_ref=normed.at[tp],
-            send_sem=ag_send.at[r],
-            recv_sem=ag_recv.at[r],
-            device_id={"tp": (tp + r) % n_tp},
-            device_id_type=MESH,
-        )
-
-    groups = 4
-    chips = n_z // groups
-    per = 2 * chips
-    half_rows = per * cap
-    step = min(512, width)
-    across = n_tp - 1 - tp
-
-    def swap(o):
-        return pltpu.make_async_remote_copy(
-            src_ref=in_buf.at[pl.ds(2 * o, 2)],
-            dst_ref=peer_buf.at[pl.ds(2 * o, 2)],
-            send_sem=swap_send.at[o],
-            recv_sem=swap_recv.at[o],
-            device_id={"tp": across},
-            device_id_type=MESH,
-        )
-
-    def pass_on(first, end):
-        @pl.loop(first, min(end, last))
-        def _(o):
-            for k in range(2):
-                token_arrival(o, k).wait_recv()
-            swap(o).start()
-
-        if end == n_z:
-            token_arrival(last, 1 - core).wait_recv()
-            swap(last).start()
-
-    def partial_copy(g):
-        return pltpu.make_async_remote_copy(
-            src_ref=part_out.at[g],
-            dst_ref=part_back.at[g],
-            send_sem=back_send.at[g],
-            recv_sem=back_recv.at[g],
-            device_id={"tp": across},
-            device_id_type=MESH,
-        )
-
-    def serve(g):
-        @pl.loop(g * chips, (g + 1) * chips)
-        def _(o):
-            swap(o).wait_recv()
-
-        mine = pl.ds(g * per, per)
-        x = jnp.concatenate(
-            [
-                peer_buf[mine].reshape(half_rows, width),
-                in_buf[mine].reshape(half_rows, width),
-            ],
-            axis=0,
-        )
-        hidden = []
-        for s in range(2):
-            gate_in = dot(x, wg[s])
-            hidden.append((gate_in / (1.0 + jnp.exp(-gate_in)) * dot(x, wu[s])).astype(BF16))
-        for c in range(0, width, step):
-            total = dot(hidden[0], wd[0, :, c : c + step]).astype(BF16).astype(F32)
-            total = total + dot(hidden[1], wd[1, :, c : c + step]).astype(BF16).astype(F32)
-            part_out[g, :, c : c + step] = total[:half_rows].astype(BF16)
-            acc[g, :, c : c + step] = total[half_rows:]
-        partial_copy(g).start()
-
-    def result_copy(o, k):
-        to = 2 * ((z + n_z - far_first(o, n_z)) % n_z) + k
-        return pltpu.make_async_remote_copy(
-            src_ref=res_buf.at[2 * o + k],
-            dst_ref=ret_buf.at[ep],
-            send_sem=ret_send.at[2 * o + k],
-            recv_sem=ret_recv.at[2 * o + core],
-            device_id={"ep": to},
-            device_id_type=MESH,
-        )
-
-    def result_arrival(o, k):
-        sender = 2 * ((z + far_first(o, n_z)) % n_z) + k
-        return pltpu.make_async_remote_copy(
-            src_ref=res_buf.at[2 * o + k],
-            dst_ref=ret_buf.at[sender],
-            send_sem=ret_send.at[2 * o + k],
-            recv_sem=ret_recv.at[2 * o + k],
-            device_id={"ep": 2 * z + 1 - core},
-            device_id_type=MESH,
-        )
-
-    sibling_back = pltpu.make_async_remote_copy(
-        src_ref=res_buf.at[2 * last + 1 - core],
-        dst_ref=ret_buf.at[ep],
-        send_sem=ret_send.at[2 * last + 1 - core],
-        recv_sem=ret_recv.at[2 * last + core],
-        device_id={"ep": 2 * z + 1 - core},
-        device_id_type=MESH,
-    )
-
-    def answer(g):
-        partial_copy(g).wait_recv()
-        res_buf[pl.ds(g * per, per)] = (
-            (acc[g] + part_back[g].astype(F32)).astype(BF16).reshape(per, cap, width)
-        )
-
-        @pl.loop(g * chips, min((g + 1) * chips, last))
-        def _(o):
-            for k in range(2):
-                result_copy(o, k).start()
-
-        if g == groups - 1:
-            sibling_back.start()
-            ret_buf[ep] = res_buf[2 * last + core]
-
-    pass_on(0, 3 * chips)
+    spread_arrival(0, across).wait_recv()
+    spreads[2].start()
+
+    each(2 * chips, 3 * chips, pass_on)
     for i in range(8, 11):
         loads[i].wait()
     for copy in shard_copies:
         copy.wait_recv()
-    for g in range(groups - 1):
-        serve(g)
-    middle = 3 * chips + chips // 2
-    pass_on(3 * chips, middle)
+    serve(0)
+    serve(1)
     answer(0)
-    pass_on(middle, n_z)
-    serve(groups - 1)
-    for r in (2, 1, 3):
-        spread(r).start()
-    for g in range(1, groups):
-        answer(g)
+    each(3 * chips, last, pass_on)
+    serve(2)
+    answer(1)
+    serve(3)
+    answer(2)
 
     for i in (3, 5, 11, 12):
         loads[i].wait()
     ext[0] = jnp.zeros((rows, ext.shape[2]), BF16)
+    for i, src in enumerate((across, beside, opposite)):
+        if i:
+            spread_arrival(i, src).wait_recv()
+        ext[src + 1] = dot(normed[src], inw_v[...]).astype(BF16)
     ext[tp + 1] = dot(normed[tp], inw_v[...]).astype(BF16)
-    for r in (1, 3, 2):
-        spread(r).wait_recv()
-        src = (tp + n_tp - r) % n_tp
-        ext[src + 1] = dot(normed[src], inw_v[...]).astype(BF16)
     window = jnp.left_shift(jnp.int32(2), tp)
     lag = lax.broadcasted_iota(jnp.int32, (rows, rows), 0) - lax.broadcasted_iota(
         jnp.int32, (rows, rows), 1
@@ -361,19 +378,18 @@
     halo.wait_recv()
     ext[0, edge, :] = jnp.where(ep == 0, 0.0, edge_in[...].astype(F32)).astype(BF16)
 
-    def sums(r):
-        to = (tp + r) % n_tp
-        return pltpu.make_async_remote_copy(
-            src_ref=part_buf.at[to],
-            dst_ref=part_in.at[r - 1],
-            send_sem=rs_send.at[r],
-            recv_sem=rs_recv.at[r],
+    def sums(i, src, to):
+        return pltpu.make_async_remote_copy(
+            src_ref=part_buf.at[src],
+            dst_ref=part_in.at[i],
+            send_sem=rs_send.at[i],
+            recv_sem=rs_recv.at[i],
             device_id={"tp": to},
             device_id_type=MESH,
         )
 
-    for r in (2, 1, 3, 0):
-        m = (tp + r) % n_tp
+    parts = [sums(0, beside, beside), sums(1, opposite, beside), sums(2, across, across)]
+    for i, m in ((1, opposite), (0, beside), (2, across), (3, tp)):
         here = ext[m + 1]
         total = dot(band, here) + dot(band_before, ext[m])
         counts = jnp.minimum(place_in + (ep * n_tp + m) * rows, window).astype(F32)
@@ -381,15 +397,19 @@
         grouped = (dot(pooled, gw_v[...]) * scale[...].astype(F32)[None]).astype(BF16)
         for c in range(0, width, step):
             part_buf[m, :, c : c + step] = dot(grouped, ow_v[:, c : c + step]).astype(BF16)
-        if r:
-            sums(r).start()
-
-    for r in (1, 3, 2):
-        sums(r).wait_recv()
-    total = part_buf[tp].astype(F32)
-    for r in range(n_tp - 1):
-        total = total + part_in[r].astype(F32)
-    mixed_out[...] = total.astype(BF16)
+        if i < 2:
+            parts[i].start()
+
+    answer(3)
+
+    parts[1].wait_recv()
+    part_buf[across] = (part_buf[across].astype(F32) + part_in[1].astype(F32)).astype(BF16)
+    parts[2].start()
+    parts[0].wait_recv()
+    parts[2].wait_recv()
+    mixed_out[...] = (
+        part_buf[tp].astype(F32) + part_in[0].astype(F32) + part_in[2].astype(F32)
+    ).astype(BF16)
 
     ids = jnp.transpose(ids_t[...])
     shares = jnp.transpose(shares_t[...])
@@ -407,11 +427,11 @@
         picks.append(jnp.where(slots == target, 1.0, 0.0).astype(BF16))
     weight = shares / jnp.sum(shares, axis=1, keepdims=True)
 
-    @pl.loop(0, last)
-    def _(o):
+    def await_results(o):
         for k in range(2):
             result_arrival(o, k).wait_recv()
 
+    each(0, last, await_results)
     pltpu.make_async_remote_copy(
         src_ref=res_buf.at[2 * last + 1 - core],
         dst_ref=ret_buf.at[2 * z + 1 - core],
@@ -429,12 +449,13 @@
     for copy in (*shard_copies, sibling, sibling_back):
         copy.wait_send()
 
-    @pl.loop(0, last)
-    def _(o):
+    def await_sent(o):
         for k in range(2):
             token_copy(o, k).wait_send()
             result_copy(o, k).wait_send()
 
+    each(0, last, await_sent)
+
     @pl.loop(0, n_z)
     def _(o):
         swap(o).wait_send()
@@ -442,9 +463,8 @@
     for g in range(groups):
         partial_copy(g).wait_send()
 
-    for r in range(1, n_tp):
-        spread(r).wait_send()
-        sums(r).wait_send()
+    for copy in (*spreads, *parts):
+        copy.wait_send()
     halo.wait_send()
 
     @pl.when(tp == n_tp - 1)

time: 256 us -> 218 us (0.85)
  Pallas kernels: 252 us -> 215 us
    pallas_call x1, Pallas kernels: 252 us -> 215 us  [local(): pl.pallas_call(functools.partial(kernel, n_ep, n_tp, cap), out_shape=(out...]
where the time goes in v4:
time: 218 us
  Pallas kernels  215 us (99%)
    pallas_call x1, Pallas kernels, local(): pl.pallas_call(functools.partial(kernel, n_ep, n_tp, cap), out_shape=(out...  215 us

profile of v4, /device:TPU:45, one launch (start us, length us, event | category | flops | bytes accessed | tf_op | source)
XLA Modules:
  0.0 217.5 jit_solution(12069629199726821135)
XLA Ops:
  0.6 215.3 %shard_map.140 = (bf16[128,2048]{1,0:T(8,128)(2,1)S(1)}, bf16[128,2048]{1,0:T(8,128)(2,1)S(1)}) custom-call(bf16[128,2048]{1,0:T(8,128)(2,1)} %mtok.1, bf16[2048]{0:T(1024)(128)(2,1)} %mgain_h.1, bf16[2048,512]{1,0:T(8,128)(2,1)} %inw.1, bf16[1,512,512]{2,1,0:T(8,128)(2,1)} %gw.1, bf16[512]{0:T(512)(128)(2,1)} %scale_h.1, bf16[512,2048]{1,0:T(8,128)(2,1)} %ow.1, ...), custom_call_target="tpu_custom_call" | custom-call | tf_op jit(solution)/shard_map/pallas_call | solution.py:493
  215.9 0.8 copy.17
  216.7 0.8 copy.18

commit v5 on v4

--- a/solution.py
+++ b/solution.py
@@ -24,7 +24,7 @@
 
 
 def offset(j, n):
-    if not isinstance(j, int):
+    if not isinstance(j, int) or j < n - 4:
         pair, i = j // 4, j % 4
         hops = (1 - i // 2) * (n // 2 - 1 - pair) + (i // 2) * (1 + pair)
         return (n + (1 - 2 * (i % 2)) * hops) % n
@@ -36,9 +36,9 @@
     mtok, mgain_h, inw, gw, scale_h, ow, etok_h, egain_h, ids_h, shares_h, gate, up, down,
     mixed_out, expert_out,
     etok, egain, mgain, scale, ids_t, shares_t,
-    xin, out_buf, in_buf, peer_buf, res_buf, ret_buf, acc, part_out, part_back, wg, wu, wd,
+    xin, meta, own_buf, stream, meta_in, relay, in_buf, peer_buf, res_buf, ret_buf, hidden, acc, part_out, part_back, wg, wu, wd,
     mrows, normed, tail, edge_out, edge_in, inw_v, gw_v, ow_v, ext, part_buf, part_in,
-    load_sem, tok_send, tok_recv, swap_send, swap_recv, back_send, back_recv,
+    load_sem, stream_send, stream_recv, tok_send, tok_recv, swap_send, swap_recv, back_send, back_recv,
     ret_send, ret_recv, w_send, w_recv,
     ag_send, ag_recv, tail_send, tail_recv, halo_send, halo_recv, rs_send, rs_recv,
 ):
@@ -121,18 +121,25 @@
         + jnp.sum(jnp.where(firsts[k], before, 0.0), axis=0, keepdims=True).astype(jnp.int32)
         for k in range(2)
     ]
-    group = min(8, n_ep)
-
-    @pl.loop(0, n_ep // group)
-    def _(q):
-        slots = lax.broadcasted_iota(jnp.int32, (group * cap, rows), 0) + q * group * cap
-        place = jnp.where((slots == targets_t[0]) | (slots == targets_t[1]), 1.0, 0.0).astype(BF16)
-        out_buf[pl.ds(q * group, group)] = (
-            dot(place, xin[...]).astype(BF16).reshape(group, cap, width)
-        )
-
+    for k in range(2):
+        meta[k : k + 1, :] = targets_t[k].astype(F32)
+
+    def pick(tokens, targets, first, count):
+        place = lax.broadcasted_iota(jnp.int32, (count * cap, rows), 0) + first * cap
+        place = jnp.where(place >= n_slots, place - n_slots, place).astype(F32)
+        chosen = jnp.where(
+            (place == targets[0:1, :]) | (place == targets[1:2, :]), 1.0, 0.0
+        ).astype(BF16)
+        return lambda c: dot(chosen, tokens[:, c : c + step]).astype(BF16).reshape(count, cap, step)
+
+    step = min(512, width)
+    own = pick(xin, meta[...], 2 * z, 2)
+    for c in range(0, width, step):
+        own_buf[:, :, c : c + step] = own(c)
     last = n_z - 1
-    in_buf[2 * last + core] = out_buf[ep]
+    in_buf[2 * last + core] = own_buf[core]
+    order = [offset(o, n_z) for o in range(n_z)]
+    ahead = [(z + 1) % n_z, (z + n_z - 1) % n_z]
 
     def each(first, end, work):
         if first < n_z - 4:
@@ -140,12 +147,44 @@
         for o in range(max(first, n_z - 4), min(end, last)):
             work(o)
 
+    def along(side, i, src, dst):
+        return pltpu.make_async_remote_copy(
+            src_ref=src,
+            dst_ref=dst,
+            send_sem=stream_send.at[2 * side + i],
+            recv_sem=stream_recv.at[2 * side + i],
+            device_id={"ep": 2 * ahead[side] + core},
+            device_id_type=MESH,
+        )
+
+    streams = [
+        copy
+        for side in range(2)
+        for copy in (
+            along(side, 0, meta, meta_in.at[side]),
+            along(side, 1, xin, stream.at[side]),
+        )
+    ]
+
     pl.semaphore_wait(barrier, n_ep - 1 + n_tp - 1)
 
-    def token_copy(o, k):
-        to = 2 * ((z + offset(o, n_z)) % n_z) + k
-        return pltpu.make_async_remote_copy(
-            src_ref=out_buf.at[to],
+    for copy in streams:
+        copy.start()
+
+    def to_sibling(o, src):
+        return pltpu.make_async_remote_copy(
+            src_ref=src,
+            dst_ref=in_buf.at[2 * o + core],
+            send_sem=tok_send.at[2 * o + 1 - core],
+            recv_sem=tok_recv.at[2 * o + core],
+            device_id={"ep": 2 * z + 1 - core},
+            device_id_type=MESH,
+        )
+
+    def relayed(o, k, side, block):
+        to = 2 * ((z + order[o] + n_z + (-1, 1)[side]) % n_z) + k
+        return pltpu.make_async_remote_copy(
+            src_ref=relay.at[side, block],
             dst_ref=in_buf.at[2 * o + core],
             send_sem=tok_send.at[2 * o + k],
             recv_sem=tok_recv.at[2 * o + core],
@@ -163,21 +202,22 @@
             device_id_type=MESH,
         )
 
-    sibling = pltpu.make_async_remote_copy(
-        src_ref=out_buf.at[2 * z + 1 - core],
-        dst_ref=in_buf.at[2 * last + core],
-        send_sem=tok_send.at[2 * last + 1 - core],
-        recv_sem=tok_recv.at[2 * last + core],
-        device_id={"ep": 2 * z + 1 - core},
-        device_id_type=MESH,
-    )
-    sibling.start()
-
-    def send_tokens(o):
+    half = n_z // 2
+    blocks = n_z - 1
+    near = [order.index(1), order.index(n_z - 1)]
+    here_at = [0, blocks - 2]
+    relays = [[], []]
+    for o in range(last):
+        d = order[o]
         for k in range(2):
-            token_copy(o, k).start()
-
-    each(0, last, send_tokens)
+            if 2 <= d < half or (d == half and k == 0):
+                relays[0].append(relayed(o, k, 0, 2 * (d - 1) + k))
+            elif half < d <= n_z - 2 or d == half:
+                relays[1].append(relayed(o, k, 1, 2 * (half - (n_z - d)) + k - 1))
+    siblings = [to_sibling(last, own_buf.at[1 - core])] + [
+        to_sibling(near[side], relay.at[side, here_at[side] + 1 - core]) for side in range(2)
+    ]
+    siblings[0].start()
     shard_copies[0].start()
 
     loads[4].wait()
@@ -228,7 +268,6 @@
     chips = n_z // groups
     per = 2 * chips
     half_rows = per * cap
-    step = min(512, width)
 
     def swap(o):
         return pltpu.make_async_remote_copy(
@@ -241,21 +280,43 @@
         )
 
     def pass_on(o):
-        for k in range(2):
-            token_arrival(o, k).wait_recv()
+        if o in near or o == last:
+            token_arrival(o, 1 - core).wait_recv()
+        else:
+            for k in range(2):
+                token_arrival(o, k).wait_recv()
         swap(o).start()
 
-    def partial_copy(g):
-        return pltpu.make_async_remote_copy(
-            src_ref=part_out.at[g],
-            dst_ref=part_back.at[g],
-            send_sem=back_send.at[g],
-            recv_sem=back_recv.at[g],
+    def pass_all(first, end):
+        for o in range(first, end):
+            pass_on(o)
+
+    pass_on(last)
+    for side in range(2):
+        arrived = [along(side, 0, meta, meta_in.at[side]), along(side, 1, xin, stream.at[side])]
+        for copy in arrived:
+            copy.wait_recv()
+        first = (2 * z, (2 * (z + 1 + half) + 1) % n_ep)[side]
+        rows_of = pick(stream.at[side], meta_in[side], first, blocks)
+        for c in range(0, width, step):
+            relay[side, :, :, c : c + step] = rows_of(c)
+        for copy in relays[side]:
+            copy.start()
+        siblings[1 + side].start()
+        in_buf[2 * near[side] + core] = relay[side, here_at[side] + core]
+
+    def partial_copy(o):
+        mine = pl.ds(o % chips * 2 * cap, 2 * cap)
+        return pltpu.make_async_remote_copy(
+            src_ref=part_out.at[o // chips, mine],
+            dst_ref=part_back.at[o // chips, mine],
+            send_sem=back_send.at[o],
+            recv_sem=back_recv.at[o],
             device_id={"tp": across},
             device_id_type=MESH,
         )
 
-    def serve(g):
+    def hide(g):
         @pl.loop(g * chips, (g + 1) * chips)
         def _(o):
             swap(o).wait_recv()
@@ -268,16 +329,18 @@
             ],
             axis=0,
         )
-        hidden = []
         for s in range(2):
             gate_in = dot(x, wg[s])
-            hidden.append((gate_in / (1.0 + jnp.exp(-gate_in)) * dot(x, wu[s])).astype(BF16))
+            hidden[g, s] = (gate_in / (1.0 + jnp.exp(-gate_in)) * dot(x, wu[s])).astype(BF16)
+
+    def lower(g):
         for c in range(0, width, step):
-            total = dot(hidden[0], wd[0, :, c : c + step]).astype(BF16).astype(F32)
-            total = total + dot(hidden[1], wd[1, :, c : c + step]).astype(BF16).astype(F32)
+            total = dot(hidden[g, 0], wd[0, :, c : c + step]).astype(BF16).astype(F32)
+            total = total + dot(hidden[g, 1], wd[1, :, c : c + step]).astype(BF16).astype(F32)
             part_out[g, :, c : c + step] = total[:half_rows].astype(BF16)
             acc[g, :, c : c + step] = total[half_rows:]
-        partial_copy(g).start()
+        for o in range(g * chips, (g + 1) * chips):
+            partial_copy(o).start()
 
     def result_copy(o, k):
         to = 2 * ((z + n_z - offset(o, n_z)) % n_z) + k
@@ -311,23 +374,21 @@
     )
 
     def answer(g):
-        partial_copy(g).wait_recv()
-        res_buf[pl.ds(g * per, per)] = (
-            (acc[g] + part_back[g].astype(F32)).astype(BF16).reshape(per, cap, width)
-        )
-
-        def send_results(o):
+        for o in range(g * chips, (g + 1) * chips):
+            partial_copy(o).wait_recv()
+            mine = pl.ds(o % chips * 2 * cap, 2 * cap)
+            res_buf[pl.ds(2 * o, 2)] = (
+                (acc[g, mine] + part_back[g, mine].astype(F32)).astype(BF16).reshape(2, cap, width)
+            )
             for k in range(2):
-                result_copy(o, k).start()
-
-        each(g * chips, (g + 1) * chips, send_results)
+                if o < last:
+                    result_copy(o, k).start()
+
         if g == groups - 1:
             sibling_back.start()
             ret_buf[ep] = res_buf[2 * last + core]
 
-    token_arrival(last, 1 - core).wait_recv()
-    swap(last).start()
-    each(0, 2 * chips, pass_on)
+    pass_all(0, 2 * chips)
 
     @pl.when(tp != n_tp - 1)
     def _():
@@ -346,18 +407,23 @@
     spread_arrival(0, across).wait_recv()
     spreads[2].start()
 
-    each(2 * chips, 3 * chips, pass_on)
+    pass_all(2 * chips, 3 * chips)
     for i in range(8, 11):
         loads[i].wait()
-    for copy in shard_copies:
+    for copy in shard_copies[:2]:
         copy.wait_recv()
-    serve(0)
-    serve(1)
+    hide(0)
+    hide(1)
+    shard_copies[2].wait_recv()
+    lower(0)
+    lower(1)
     answer(0)
-    each(3 * chips, last, pass_on)
-    serve(2)
+    pass_all(3 * chips, last)
+    hide(2)
+    lower(2)
     answer(1)
-    serve(3)
+    hide(3)
+    lower(3)
     answer(2)
 
     for i in (3, 5, 11, 12):
@@ -446,12 +512,11 @@
         mix = dot(picks[0], back) * weight[:, 0:1] + dot(picks[1], back) * weight[:, 1:2]
         expert_out[:, c : c + step] = mix.astype(BF16)
 
-    for copy in (*shard_copies, sibling, sibling_back):
+    for copy in (*shard_copies, *streams, *relays[0], *relays[1], *siblings, sibling_back):
         copy.wait_send()
 
     def await_sent(o):
         for k in range(2):
-            token_copy(o, k).wait_send()
             result_copy(o, k).wait_send()
 
     each(0, last, await_sent)
@@ -460,8 +525,8 @@
     def _(o):
         swap(o).wait_send()
 
-    for g in range(groups):
-        partial_copy(g).wait_send()
+    for o in range(n_z):
+        partial_copy(o).wait_send()
 
     for copy in (*spreads, *parts):
         copy.wait_send()
@@ -503,11 +568,16 @@
                 V((2, rows), jnp.int32),
                 V((2, rows), F32),
                 V((rows, width), BF16),
+                V((2, rows), F32),
+                V((2, cap, width), BF16),
+                V((2, rows, width), BF16),
+                V((2, 2, rows), F32),
+                V((2, n_ep // 2 - 1, cap, width), BF16),
                 V((n_ep, cap, width), BF16),
                 V((n_ep, cap, width), BF16),
                 V((n_ep, cap, width), BF16),
                 V((n_ep, cap, width), BF16),
-                V((n_ep, cap, width), BF16),
+                V((4, 2, slots // 2, ff), BF16),
                 V((4, slots // 4, width), F32),
                 V((4, slots // 4, width), BF16),
                 V((4, slots // 4, width), BF16),
@@ -526,12 +596,14 @@
                 V((n_tp, rows, width), BF16),
                 V((n_tp - 1, rows, width), BF16),
                 dma((13,)),
+                dma((4,)),
+                dma((4,)),
                 dma((n_ep,)),
                 dma((n_ep,)),
                 dma((n_ep // 2,)),
                 dma((n_ep // 2,)),
-                dma((4,)),
-                dma((4,)),
+                dma((n_ep // 2,)),
+                dma((n_ep // 2,)),
                 dma((n_ep,)),
                 dma((n_ep,)),
                 dma((3,)),

time: 218 us -> 210 us (0.963)
  Pallas kernels: 215 us -> 206 us
    pallas_call x1, Pallas kernels: 215 us -> 206 us  [local(): pl.pallas_call(functools.partial(kernel, n_ep, n_tp, cap), out_shape=(out...]
where the time goes in v5:
time: 210 us; the launch traced here: 208 us
  Pallas kernels  206 us (98%)
    pallas_call x1, Pallas kernels, local(): pl.pallas_call(functools.partial(kernel, n_ep, n_tp, cap), out_shape=(out...  206 us

profile of v5, /device:TPU:45, one launch (start us, length us, event | category | flops | bytes accessed | tf_op | source)
XLA Modules:
  0.0 208.1 jit_solution(17150295048741684778)
XLA Ops:
  0.6 205.8 %shard_map.140 = (bf16[128,2048]{1,0:T(8,128)(2,1)S(1)}, bf16[128,2048]{1,0:T(8,128)(2,1)S(1)}) custom-call(bf16[128,2048]{1,0:T(8,128)(2,1)} %mtok.1, bf16[2048]{0:T(1024)(128)(2,1)} %mgain_h.1, bf16[2048,512]{1,0:T(8,128)(2,1)} %inw.1, bf16[1,512,512]{2,1,0:T(8,128)(2,1)} %gw.1, bf16[512]{0:T(512)(128)(2,1)} %scale_h.1, bf16[512,2048]{1,0:T(8,128)(2,1)} %ow.1, ...), custom_call_target="tpu_custom_call" | custom-call | tf_op jit(solution)/shard_map/pallas_call | solution.py:558
  206.5 0.8 copy.17
  207.3 0.8 copy.18

commit v6 on v5

--- a/solution.py
+++ b/solution.py
@@ -36,10 +36,10 @@
     mtok, mgain_h, inw, gw, scale_h, ow, etok_h, egain_h, ids_h, shares_h, gate, up, down,
     mixed_out, expert_out,
     etok, egain, mgain, scale, ids_t, shares_t,
-    xin, meta, own_buf, stream, meta_in, relay, in_buf, peer_buf, res_buf, ret_buf, hidden, acc, part_out, part_back, wg, wu, wd,
+    xin, meta, own_buf, stream, meta_in, relay, in_buf, peer_buf, res_buf, back, own_back, sums_out, home, hidden, acc, part_out, part_back, wg, wu, wd,
     mrows, normed, tail, edge_out, edge_in, inw_v, gw_v, ow_v, ext, part_buf, part_in,
     load_sem, stream_send, stream_recv, tok_send, tok_recv, swap_send, swap_recv, back_send, back_recv,
-    ret_send, ret_recv, w_send, w_recv,
+    ret_send, ret_recv, home_send, home_recv, w_send, w_recv,
     ag_send, ag_recv, tail_send, tail_recv, halo_send, halo_recv, rs_send, rs_recv,
 ):
     ep = lax.axis_index("ep")
@@ -86,7 +86,7 @@
     ]
     for load in loads:
         load.start()
-    for i in range(3):
+    for i in range(4):
         loads[i].wait()
 
     def weights(i, src, dst):
@@ -123,6 +123,8 @@
     ]
     for k in range(2):
         meta[k : k + 1, :] = targets_t[k].astype(F32)
+    weight = shares_t[...]
+    meta[2:4, :] = weight / jnp.sum(weight, axis=0, keepdims=True)
 
     def pick(tokens, targets, first, count):
         place = lax.broadcasted_iota(jnp.int32, (count * cap, rows), 0) + first * cap
@@ -141,12 +143,6 @@
     order = [offset(o, n_z) for o in range(n_z)]
     ahead = [(z + 1) % n_z, (z + n_z - 1) % n_z]
 
-    def each(first, end, work):
-        if first < n_z - 4:
-            pl.loop(first, min(end, n_z - 4))(work)
-        for o in range(max(first, n_z - 4), min(end, last)):
-            work(o)
-
     def along(side, i, src, dst):
         return pltpu.make_async_remote_copy(
             src_ref=src,
@@ -206,6 +202,7 @@
     blocks = n_z - 1
     near = [order.index(1), order.index(n_z - 1)]
     here_at = [0, blocks - 2]
+    firsts_at = [2 * z, (2 * (z + 1 + half) + 1) % n_ep]
     relays = [[], []]
     for o in range(last):
         d = order[o]
@@ -296,8 +293,7 @@
         arrived = [along(side, 0, meta, meta_in.at[side]), along(side, 1, xin, stream.at[side])]
         for copy in arrived:
             copy.wait_recv()
-        first = (2 * z, (2 * (z + 1 + half) + 1) % n_ep)[side]
-        rows_of = pick(stream.at[side], meta_in[side], first, blocks)
+        rows_of = pick(stream.at[side], meta_in[side], firsts_at[side], blocks)
         for c in range(0, width, step):
             relay[side, :, :, c : c + step] = rows_of(c)
         for copy in relays[side]:
@@ -343,35 +339,45 @@
             partial_copy(o).start()
 
     def result_copy(o, k):
-        to = 2 * ((z + n_z - offset(o, n_z)) % n_z) + k
+        d = order[o]
+        origin = z + n_z - d
+        if d == half:
+            side, block, to = core, (1 - core) * (blocks - 1), origin + 1 - 2 * core
+        elif d < half:
+            side, block, to = 0, 2 * (d - 1) + core, origin + 1
+        else:
+            side, block, to = 1, 2 * (half - (n_z - d)) + core - 1, origin - 1
         return pltpu.make_async_remote_copy(
             src_ref=res_buf.at[2 * o + k],
-            dst_ref=ret_buf.at[ep],
+            dst_ref=back.at[side, block],
             send_sem=ret_send.at[2 * o + k],
-            recv_sem=ret_recv.at[2 * o + core],
-            device_id={"ep": to},
-            device_id_type=MESH,
-        )
-
-    def result_arrival(o, k):
-        sender = 2 * ((z + offset(o, n_z)) % n_z) + k
-        return pltpu.make_async_remote_copy(
-            src_ref=res_buf.at[2 * o + k],
-            dst_ref=ret_buf.at[sender],
-            send_sem=ret_send.at[2 * o + k],
-            recv_sem=ret_recv.at[2 * o + k],
+            recv_sem=ret_recv.at[side * blocks + block],
+            device_id={"ep": 2 * (to % n_z) + k},
+            device_id_type=MESH,
+        )
+
+    def result_to_sibling(o, dst, sem):
+        return pltpu.make_async_remote_copy(
+            src_ref=res_buf.at[2 * o + 1 - core],
+            dst_ref=dst,
+            send_sem=ret_send.at[2 * o + 1 - core],
+            recv_sem=ret_recv.at[sem],
             device_id={"ep": 2 * z + 1 - core},
             device_id_type=MESH,
         )
 
-    sibling_back = pltpu.make_async_remote_copy(
-        src_ref=res_buf.at[2 * last + 1 - core],
-        dst_ref=ret_buf.at[ep],
-        send_sem=ret_send.at[2 * last + 1 - core],
-        recv_sem=ret_recv.at[2 * last + core],
-        device_id={"ep": 2 * z + 1 - core},
-        device_id_type=MESH,
-    )
+    def result_arrival(dst, sem):
+        return result_to_sibling(last, dst, sem)
+
+    results = {
+        o: [result_copy(o, k) for k in range(2)] for o in range(last) if o not in near
+    }
+    for side in range(2):
+        block = here_at[side] + core
+        results[near[side]] = [
+            result_to_sibling(near[side], back.at[side, block], side * blocks + block)
+        ]
+    results[last] = [result_to_sibling(last, own_back.at[core], 2 * blocks + core)]
 
     def answer(g):
         for o in range(g * chips, (g + 1) * chips):
@@ -380,13 +386,14 @@
             res_buf[pl.ds(2 * o, 2)] = (
                 (acc[g, mine] + part_back[g, mine].astype(F32)).astype(BF16).reshape(2, cap, width)
             )
-            for k in range(2):
-                if o < last:
-                    result_copy(o, k).start()
+            for copy in results[o]:
+                copy.start()
+            if o in near:
+                side = near.index(o)
+                back[side, here_at[side] + core] = res_buf[2 * o + core]
 
         if g == groups - 1:
-            sibling_back.start()
-            ret_buf[ep] = res_buf[2 * last + core]
+            own_back[core] = res_buf[2 * last + core]
 
     pass_all(0, 2 * chips)
 
@@ -426,7 +433,7 @@
     lower(3)
     answer(2)
 
-    for i in (3, 5, 11, 12):
+    for i in (5, 11, 12):
         loads[i].wait()
     ext[0] = jnp.zeros((rows, ext.shape[2]), BF16)
     for i, src in enumerate((across, beside, opposite)):
@@ -477,49 +484,62 @@
         part_buf[tp].astype(F32) + part_in[0].astype(F32) + part_in[2].astype(F32)
     ).astype(BF16)
 
-    ids = jnp.transpose(ids_t[...])
-    shares = jnp.transpose(shares_t[...])
-    lanes = lax.broadcasted_iota(jnp.int32, (rows, n_ep), 1)
-    mine = [ids[:, k : k + 1] == lanes for k in range(2)]
-    named_rows = jnp.where(mine[0] | mine[1], 1.0, 0.0).astype(BF16)
-    later = jnp.where(lag > 0, 1.0, 0.0).astype(BF16)
-    before_rows = dot(later, named_rows)
-    slots = lax.broadcasted_iota(jnp.int32, (rows, n_slots), 1)
-    picks = []
-    for k in range(2):
-        target = ids[:, k : k + 1] * cap + jnp.sum(
-            jnp.where(mine[k], before_rows, 0.0), axis=1, keepdims=True
-        ).astype(jnp.int32)
-        picks.append(jnp.where(slots == target, 1.0, 0.0).astype(BF16))
-    weight = shares / jnp.sum(shares, axis=1, keepdims=True)
-
-    def await_results(o):
-        for k in range(2):
-            result_arrival(o, k).wait_recv()
-
-    each(0, last, await_results)
-    pltpu.make_async_remote_copy(
-        src_ref=res_buf.at[2 * last + 1 - core],
-        dst_ref=ret_buf.at[2 * z + 1 - core],
-        send_sem=ret_send.at[2 * last + 1 - core],
-        recv_sem=ret_recv.at[2 * last + 1 - core],
-        device_id={"ep": 2 * z + 1 - core},
-        device_id_type=MESH,
-    ).wait_recv()
-
-    for c in range(0, width, step):
-        back = ret_buf[:, :, c : c + step].reshape(n_slots, step)
-        mix = dot(picks[0], back) * weight[:, 0:1] + dot(picks[1], back) * weight[:, 1:2]
-        expert_out[:, c : c + step] = mix.astype(BF16)
-
-    for copy in (*shard_copies, *streams, *relays[0], *relays[1], *siblings, sibling_back):
+    def mixed_rows(told, first, count):
+        told = jnp.transpose(told)
+        place = lax.broadcasted_iota(jnp.int32, (rows, count * cap), 1) + first * cap
+        place = jnp.where(place >= n_slots, place - n_slots, place).astype(F32)
+        picks = [jnp.where(place == told[:, k : k + 1], 1.0, 0.0).astype(BF16) for k in range(2)]
+        return lambda found: (
+            dot(picks[0], found) * told[:, 2:3] + dot(picks[1], found) * told[:, 3:4]
+        )
+
+    def homeward(side, h):
+        return pltpu.make_async_remote_copy(
+            src_ref=sums_out.at[side, h],
+            dst_ref=home.at[side, h],
+            send_sem=home_send.at[2 * side + h],
+            recv_sem=home_recv.at[2 * side + h],
+            device_id={"ep": 2 * ahead[1 - side] + core},
+            device_id_type=MESH,
+        )
+
+    wide = width // 2
+    part_step = min(step, wide)
+    for side in range(2):
+        for block in range(blocks):
+            if block not in (here_at[side], here_at[side] + 1):
+                result_arrival(back.at[side, block], side * blocks + block).wait_recv()
+        block = here_at[side] + 1 - core
+        result_arrival(back.at[side, block], side * blocks + block).wait_recv()
+        weigh = mixed_rows(meta_in[side], firsts_at[side], blocks)
+        for h in range(2):
+            for c in range(0, wide, part_step):
+                at = h * wide + c
+                found = back[side, :, :, at : at + part_step].reshape(blocks * cap, part_step)
+                sums_out[side, h, :, c : c + part_step] = weigh(found).astype(BF16)
+            homeward(side, h).start()
+
+    result_arrival(own_back.at[1 - core], 2 * blocks + 1 - core).wait_recv()
+    weigh = mixed_rows(meta[...], 2 * z, 2)
+    for h in range(2):
+        for side in range(2):
+            homeward(side, h).wait_recv()
+        for c in range(0, wide, part_step):
+            at = h * wide + c
+            total = weigh(own_back[:, :, at : at + part_step].reshape(2 * cap, part_step))
+            for side in range(2):
+                total = total + home[side, h, :, c : c + part_step].astype(F32)
+            expert_out[:, at : at + part_step] = total.astype(BF16)
+
+    for copy in (*shard_copies, *streams, *relays[0], *relays[1], *siblings):
         copy.wait_send()
 
-    def await_sent(o):
-        for k in range(2):
-            result_copy(o, k).wait_send()
-
-    each(0, last, await_sent)
+    for o in range(n_z):
+        for copy in results[o]:
+            copy.wait_send()
+    for side in range(2):
+        for h in range(2):
+            homeward(side, h).wait_send()
 
     @pl.loop(0, n_z)
     def _(o):
@@ -568,15 +588,18 @@
                 V((2, rows), jnp.int32),
                 V((2, rows), F32),
                 V((rows, width), BF16),
-                V((2, rows), F32),
+                V((4, rows), F32),
                 V((2, cap, width), BF16),
                 V((2, rows, width), BF16),
-                V((2, 2, rows), F32),
+                V((2, 4, rows), F32),
                 V((2, n_ep // 2 - 1, cap, width), BF16),
                 V((n_ep, cap, width), BF16),
                 V((n_ep, cap, width), BF16),
                 V((n_ep, cap, width), BF16),
-                V((n_ep, cap, width), BF16),
+                V((2, n_ep // 2 - 1, cap, width), BF16),
+                V((2, cap, width), BF16),
+                V((2, 2, rows, width // 2), BF16),
+                V((2, 2, rows, width // 2), BF16),
                 V((4, 2, slots // 2, ff), BF16),
                 V((4, slots // 4, width), F32),
                 V((4, slots // 4, width), BF16),
@@ -606,6 +629,8 @@
                 dma((n_ep // 2,)),
                 dma((n_ep,)),
                 dma((n_ep,)),
+                dma((4,)),
+                dma((4,)),
                 dma((3,)),
                 dma((3,)),
                 dma((n_tp,)),

time: 210 us -> 200 us (0.952)
  Pallas kernels: 206 us -> 197 us
    pallas_call x1, Pallas kernels: 206 us -> 197 us  [local(): pl.pallas_call(functools.partial(kernel, n_ep, n_tp, cap), out_shape=(out...]
where the time goes in v6:
time: 200 us
  Pallas kernels  197 us (98%)
    pallas_call x1, Pallas kernels, local(): pl.pallas_call(functools.partial(kernel, n_ep, n_tp, cap), out_shape=(out...  197 us

profile of v6, /device:TPU:45, one launch (start us, length us, event | category | flops | bytes accessed | tf_op | source)
XLA Modules:
  0.0 199.7 jit_solution(12701599096474610611)
XLA Ops:
  0.6 197.4 %shard_map.140 = (bf16[128,2048]{1,0:T(8,128)(2,1)S(1)}, bf16[128,2048]{1,0:T(8,128)(2,1)S(1)}) custom-call(bf16[128,2048]{1,0:T(8,128)(2,1)} %mtok.1, bf16[2048]{0:T(1024)(128)(2,1)} %mgain_h.1, bf16[2048,512]{1,0:T(8,128)(2,1)} %inw.1, bf16[1,512,512]{2,1,0:T(8,128)(2,1)} %gw.1, bf16[512]{0:T(512)(128)(2,1)} %scale_h.1, bf16[512,2048]{1,0:T(8,128)(2,1)} %ow.1, ...), custom_call_target="tpu_custom_call" | custom-call | tf_op jit(solution)/shard_map/pallas_call | solution.py:578
  198.1 0.8 copy.17
  198.9 0.8 copy.18
